TPU v7x, 128 devices: a whole 4x4x4 slice. The times are simulated.
128 devices in a mesh: sp: 64 (over z, y, x), tp: 2 (over core).
Axes of the slice: x: 4, y: 4, z: 4, core: 2. Of those that a mesh axis runs over, the one named last changes fastest.
Arguments:
- tokens: bfloat16 [24576, 2048], P(('sp', 'tp')), may hold values from -6 to 6
- norm_gain: float32 [2048], replicated, may hold values from 0.1 to 1.9
- w_query: bfloat16 [2048, 1024], P(None, 'tp'), may hold values from -0.125 to 0.125
- w_key: bfloat16 [2048, 1024], P(None, 'tp'), may hold values from -0.125 to 0.125
- w_value: bfloat16 [2048, 2048], P(None, 'tp'), may hold values from -0.125 to 0.125
- w_ogate: bfloat16 [2048, 2048], P(None, 'tp'), may hold values from -0.125 to 0.125
- w_igate: bfloat16 [2048, 8], replicated, may hold values from -0.125 to 0.125
- w_fgate: bfloat16 [2048, 8], replicated, may hold values from -0.125 to 0.125
- conv_query: bfloat16 [4, 1024], replicated, may hold values from -3 to 3
- conv_key: bfloat16 [4, 1024], replicated, may hold values from -3 to 3
- gate_offset: float32 [2, 192, 8], P(None, 'sp', 'tp'), may hold values from -60 to 140, as said below
- head_gain: float32 [2048], replicated, may hold values from 0.1 to 1.9
- w_out: bfloat16 [2048, 2048], P('tp'), may hold values from -0.125 to 0.125
Outputs:
- mixed: bfloat16 [24576, 2048], P(('sp', 'tp'))
Inputs may be any that keep to these rules, and one draw needn't show every extreme that they name: `gate_offset`: row 0 is added to the input gate's pre-activation and row 1 to the forget gate's; each entry holds for one block of 128 positions and one head.
All inputs are finite; a program needn't handle non-finite values.
Results may differ from a plain program's by a relative error of at most 0.011.
Values may be sent and summed in bfloat16 or wider, within the bound.
No kernel may reach another device: no remote copies, remote signals or barrier semaphores. Data moves between devices by JAX's collectives and lax.ppermute only.
A program may use at most 128 MiB of HBM per device.

v0:
```python
import jax
import jax.numpy as jnp
from jax import lax
from jax.sharding import Mesh
from jax.sharding import PartitionSpec as P

SPAN = 128
SP = ("sp_0", "sp_1", "sp_2")
SP_TP = ("sp_0", "sp_1", "sp_2", "tp")


EPS = 1e-06
EMPTY_LEVEL = -1e30


def nothing_yet(shard, identity):
    return jax.tree.map(
        lambda a, e: jnp.broadcast_to(jnp.asarray(e, a.dtype), a.shape), shard, identity
    )


def gathered_once(shard, axis):
    leaves = jax.tree.leaves(shard)
    order = sorted(range(len(leaves)), key=lambda k: -leaves[k].size)
    width = (1, *leaves[order[0]].shape)[-1]
    lines = [
        jnp.pad(leaves[k].reshape(-1), (0, -leaves[k].size % width)).reshape(-1, width)
        for k in order
    ]
    both, at, found = (lax.all_gather(jnp.concatenate(lines), axis), 0, {})
    for k, line in zip(order, lines):
        piece = both[:, at : at + len(line)].reshape(len(both), -1)
        found[k] = piece[:, : leaves[k].size].reshape(-1, *leaves[k].shape)
        at += len(line)
    numbers = iter(range(len(leaves)))
    return jax.tree.map(lambda _: found[next(numbers)], shard)


def carried_in(shard, axes, combine, identity):
    before = start = nothing_yet(shard, identity)
    running = shard
    for axis in reversed(axes):
        size, index = (lax.axis_size(axis), lax.axis_index(axis))
        pieces = gathered_once(running, axis)
        inside, running = (start, start)
        for k in range(size):
            passed = k < index
            running = combine(running, jax.tree.map(lambda part: part[k], pieces))
            inside = jax.tree.map(lambda new, old: jnp.where(passed, new, old), running, inside)
        before = combine(inside, before)
    return before


def sent_to_all(shard, axis):
    copies = jnp.broadcast_to(shard, (lax.axis_size(axis), *shard.shape))
    return lax.all_to_all(copies, axis, split_axis=0, concat_axis=0, tiled=True)


def joined_along(blocks, dim):
    blocks = jnp.moveaxis(blocks, 0, dim)
    dims = blocks.shape
    return blocks.reshape(*dims[:dim], dims[dim] * dims[dim + 1], *dims[dim + 2 :])


def gathered_copies(shard, axis, dim):
    blocks = sent_to_all(shard, axis)
    return joined_along(blocks, dim)


def passed_along(shard, axis, by):
    size = lax.axis_size(axis)
    pairs = [(i, i + by) for i in range(size) if 0 <= i + by < size]
    return lax.ppermute(shard, axis, pairs)


def normalize_rows(values, gain_vec):
    widened = values.astype(jnp.float32)
    scaled = widened * lax.rsqrt(jnp.mean(widened * widened, axis=-1, keepdims=True) + EPS)
    return (scaled * gain_vec).astype(jnp.bfloat16)


def causal_mix(values, leading, weight):
    tap_count = weight.shape[0]
    seq_len = values.shape[0]
    padded = jnp.concatenate([leading, values], axis=0).astype(jnp.float32)
    mixed_sum = jnp.zeros((seq_len, values.shape[1]), jnp.float32)
    for tap_index in range(tap_count):
        mixed_sum = (
            mixed_sum
            + weight[tap_index].astype(jnp.float32) * padded[tap_index : tap_index + seq_len]
        )
    return mixed_sum


def block_read(carried, cumulative, gate_rows, query_blk, key_blk, value_blk):
    states, norm_vec, levels = carried
    span_len = cumulative.shape[1]
    causal = jnp.tril(jnp.ones((span_len, span_len), dtype=bool))
    log_weight = jnp.where(
        causal[None],
        cumulative[:, :, None] - cumulative[:, None, :] + gate_rows[:, None, :],
        -jnp.inf,
    )
    carried_log = cumulative + levels[:, None]
    running_top = jnp.maximum(carried_log, jnp.max(log_weight, axis=-1))
    inner_weight = jnp.exp(log_weight - running_top[:, :, None])
    carried_scale = jnp.exp(carried_log - running_top)
    scores = (
        jnp.einsum("thd,shd->hts", query_blk, key_blk, preferred_element_type=jnp.float32)
        * inner_weight
    )
    query_wide = query_blk.astype(jnp.float32)
    numerator = carried_scale[:, :, None] * jnp.einsum("thd,hde->hte", query_wide, states)
    numerator = numerator + jnp.einsum(
        "hts,she->hte", scores.astype(jnp.bfloat16), value_blk, preferred_element_type=jnp.float32
    )
    denominator = carried_scale * jnp.einsum("thd,hd->ht", query_wide, norm_vec) + jnp.sum(
        scores, axis=-1
    )
    return (numerator, denominator, running_top)


def block_write(carried, cumulative, gate_rows, key_blk, value_blk):
    states, norm_vec, levels = carried
    last_log = cumulative[:, -1]
    write_log = last_log[:, None] - cumulative + gate_rows
    new_levels = jnp.maximum(last_log + levels, jnp.max(write_log, axis=-1))
    decay_scale = jnp.exp(last_log + levels - new_levels)
    write_weight = jnp.exp(write_log - new_levels[:, None])
    weighted = write_weight.T[:, :, None] * key_blk.astype(jnp.float32)
    new_states = decay_scale[:, None, None] * states + jnp.einsum(
        "shd,she->hde", weighted.astype(jnp.bfloat16), value_blk, preferred_element_type=jnp.float32
    )
    new_norm = decay_scale[:, None] * norm_vec + jnp.sum(weighted, axis=0)
    return (new_states, new_norm, new_levels)


def read_write(carried, inputs):
    query_blk, key_blk, value_blk, gate_blk, forget_blk = inputs
    cumulative = jnp.cumsum(forget_blk, axis=0).T
    gate_rows = gate_blk.T
    outputs = block_read(carried, cumulative, gate_rows, query_blk, key_blk, value_blk)
    return (block_write(carried, cumulative, gate_rows, key_blk, value_blk), outputs)


def write_only(carried, inputs):
    key_blk, value_blk, gate_blk, forget_blk = inputs
    cumulative = jnp.cumsum(forget_blk, axis=0).T
    return (block_write(carried, cumulative, gate_blk.T, key_blk, value_blk), None)


def join_states(earlier_part, later_part):
    forget_one, states_one, norm_one, level_one = earlier_part
    forget_two, states_two, norm_two, level_two = later_part
    shifted = level_one + forget_two
    new_level = jnp.maximum(shifted, level_two)
    scale_one = jnp.exp(shifted - new_level)
    scale_two = jnp.exp(level_two - new_level)
    new_states = scale_one[:, None, None] * states_one + scale_two[:, None, None] * states_two
    new_norm = scale_one[:, None] * norm_one + scale_two[:, None] * norm_two
    return (forget_one + forget_two, new_states, new_norm, new_level)


def pass_state(summary, blank_state):
    return carried_in(
        (summary[0], summary[1], summary[2], summary[3]),
        SP,
        join_states,
        (jnp.zeros_like(summary[0]), blank_state[0], blank_state[1], blank_state[2]),
    )


def unblock(block_parts, seq_len):
    numerator, denominator, running_top = block_parts
    local_heads = numerator.shape[1]
    numerator = jnp.transpose(numerator, (0, 2, 1, 3)).reshape(
        seq_len, local_heads, numerator.shape[3]
    )
    denominator = jnp.transpose(denominator, (0, 2, 1)).reshape(seq_len, local_heads)
    running_top = jnp.transpose(running_top, (0, 2, 1)).reshape(seq_len, local_heads)
    return (numerator, denominator, running_top)


def body(
    tokens,
    norm_gain,
    w_query,
    w_key,
    w_value,
    w_ogate,
    w_igate,
    w_fgate,
    conv_query,
    conv_key,
    gate_offset,
    head_gain,
    w_out,
):
    normed = normalize_rows(tokens, norm_gain)
    gathered = gathered_copies(normed, "tp", 0)
    seq_len = gathered.shape[0]
    local_heads = gate_offset.shape[2]
    key_dim = w_query.shape[1] // local_heads
    value_dim = w_value.shape[1] // local_heads
    head_first = lax.axis_index("tp") * local_heads
    query_pre = jnp.dot(gathered, w_query, preferred_element_type=jnp.float32).astype(jnp.bfloat16)
    key_pre = jnp.dot(gathered, w_key, preferred_element_type=jnp.float32).astype(jnp.bfloat16)
    value_pre = jnp.dot(gathered, w_value, preferred_element_type=jnp.float32).astype(jnp.bfloat16)
    ogate_pre = jnp.dot(gathered, w_ogate, preferred_element_type=jnp.float32).astype(jnp.bfloat16)
    input_cols = lax.dynamic_slice_in_dim(w_igate, head_first, local_heads, 1)
    forget_cols = lax.dynamic_slice_in_dim(w_fgate, head_first, local_heads, 1)
    input_pre = jnp.dot(gathered, input_cols, preferred_element_type=jnp.float32)
    forget_pre = jnp.dot(gathered, forget_cols, preferred_element_type=jnp.float32)
    input_gate = input_pre + jnp.repeat(gate_offset[0], SPAN, axis=0)
    log_forget = jax.nn.log_sigmoid(forget_pre + jnp.repeat(gate_offset[1], SPAN, axis=0))
    tap_count = conv_query.shape[0]
    tail_rows = jnp.stack(
        [query_pre[seq_len - tap_count + 1 :], key_pre[seq_len - tap_count + 1 :]]
    )
    before = passed_along(tail_rows, SP, 1)
    query_taps = lax.dynamic_slice_in_dim(
        conv_query, head_first * key_dim, local_heads * key_dim, 1
    )
    key_taps = lax.dynamic_slice_in_dim(conv_key, head_first * key_dim, local_heads * key_dim, 1)
    query_rows = (
        jax.nn.silu(causal_mix(query_pre, before[0], query_taps))
        .astype(jnp.bfloat16)
        .reshape(seq_len, local_heads, key_dim)
    )
    key_rows = (
        (jax.nn.silu(causal_mix(key_pre, before[1], key_taps)) * key_dim ** (-0.5))
        .astype(jnp.bfloat16)
        .reshape(seq_len, local_heads, key_dim)
    )
    value_rows = value_pre.reshape(seq_len, local_heads, value_dim)
    blocks = seq_len // SPAN
    blocked = (
        query_rows.reshape(blocks, SPAN, local_heads, key_dim),
        key_rows.reshape(blocks, SPAN, local_heads, key_dim),
        value_rows.reshape(blocks, SPAN, local_heads, value_dim),
        input_gate.reshape(blocks, SPAN, local_heads),
        log_forget.reshape(blocks, SPAN, local_heads),
    )
    blank_state = (
        jnp.zeros((local_heads, key_dim, value_dim), jnp.float32),
        jnp.zeros((local_heads, key_dim), jnp.float32),
        jnp.full((local_heads,), EMPTY_LEVEL, jnp.float32),
    )
    end_state, _ = lax.scan(write_only, blank_state, blocked[1:])
    incoming = pass_state((jnp.sum(log_forget, axis=0),) + end_state, blank_state)
    _, block_parts = lax.scan(read_write, incoming[1:], blocked)
    numerator, denominator, running_top = unblock(block_parts, seq_len)
    cell_out = numerator / jnp.maximum(jnp.abs(denominator), jnp.exp(-running_top))[:, :, None]
    cell_out = cell_out * lax.rsqrt(jnp.mean(cell_out * cell_out, axis=-1, keepdims=True) + EPS)
    gain_local = lax.dynamic_slice_in_dim(
        head_gain, head_first * value_dim, local_heads * value_dim, 0
    )
    hidden = (
        cell_out.reshape(seq_len, local_heads * value_dim)
        * gain_local
        * jax.nn.sigmoid(ogate_pre.astype(jnp.float32))
    )
    hidden = hidden.astype(jnp.bfloat16)
    by_token = lax.all_to_all(hidden, "tp", split_axis=0, concat_axis=1, tiled=True)
    full_weight = lax.all_gather(w_out, "tp", axis=0, tiled=True)
    mixed_out = jnp.dot(by_token, full_weight, preferred_element_type=jnp.float32)
    return mixed_out.astype(jnp.bfloat16)


def solution(mesh):
    split = Mesh(mesh.devices.reshape(4, 4, 4, mesh.shape["tp"]), ("sp_0", "sp_1", "sp_2", "tp"))
    placed = (
        P(SP_TP, None),
        P(),
        P(None, "tp"),
        P(None, "tp"),
        P(None, "tp"),
        P(None, "tp"),
        P(),
        P(),
        P(),
        P(),
        P(None, SP, "tp"),
        P(),
        P("tp", None),
    )
    return jax.shard_map(
        body, mesh=split, in_specs=placed, out_specs=P(SP_TP, None), check_vma=False
    )
```

profile of v0, /device:TPU:1, one launch (start us, length us, event | category | flops | bytes accessed | tf_op | source)
XLA Modules:
  0.0 191.1 jit_solution(11595736026542875786)
XLA Ops:
  6.5 1.5 fusion.32
  8.1 1.4 fusion.34
  9.7 6.0 %all_to_all.24 = bf16[2,192,2048]{2,1,0:T(8,128)(2,1)S(1)} all-to-all(bf16[2,192,2048]{2,1,0:T(8,128)(2,1)S(1)} %broadcast_in_dim.40), channel_id=1, replica_groups=mesh['sp_0'=4,'sp_1'=4,'sp_2'=4,'tp'=2] {'tp'}, dimensions={0} | all-to-all | bytes 3145728 | tf_op jit(solution)/shard_map/all_to_all | solution.py:56
  15.7 1.0 convolution_convert_fusion.3
  16.8 1.0 copy-done.22
  17.8 1.0 convolution_convert_fusion.4
  18.8 3.2 %collective-permute-start = (bf16[2,3,512]{2,1,0:T(4,128)(2,1)S(1)}, bf16[2,3,512]{2,1,0:T(4,128)(2,1)S(1)}, u32[]{:S(2)}, u32[]{:S(2)}) collective-permute-start(bf16[2,3,512]{2,1,0:T(4,128)(2,1)S(1)} %pad_maximum_fusion), channel_id=1, source_target_pairs={{0,2},{2,4},{4,6},{6,8},{8,10},{10,12},{12,14},{14,16},{16,18},{18... | collective-permute-start | bytes 18440 | tf_op jit(solution)/shard_map/ppermute | solution.py:73
  22.1 5.4 %convolution_convert_fusion.2 = bf16[384,1024]{1,0:T(8,128)(2,1)} fusion(bf16[384,2048]{1,0:T(8,128)(2,1)} %bitcast.700, bf16[2048,1024]{1,0:T(8,128)(2,1)} %param.21), kind=kOutput, calls=%fused_computation.73 | convolution fusion | flops 1611005952 | bytes 6553600 | tf_op jit(solution)/shard_map/dot_general | solution.py:208
  27.6 0.7 fusion.121
  28.3 0.5 fusion.35
  29.2 2.0 %reshape_reshape.7 = bf16[3,128,4,256]{3,2,1,0:T(4,128)(2,1)S(1)} reshape(bf16[384,1024]{1,0:T(8,128)(2,1)} %convolution_convert_fusion.2) | data formatting | bytes 1572864 | tf_op jit(solution)/shard_map/reshape;reshape | solution.py:240
  31.5 0.5 multiply_convert_fusion.2
  32.1 3.5 %while.36 = (s32[]{:T(128)}, f32[4,128,256]{2,1,0:T(8,128)S(1)}, f32[4,128]{1,0:T(4,128)S(1)}, f32[4]{0:T(128)S(1)}, f32[3,128,4]{2,1,0:T(8,128)S(1)}, /*index=5...) while((s32[]{:T(128)}, f32[4,128,256]{2,1,0:T(8,128)S(1)}, ...), condition=%wide.region_5.6_spmd.clone, body=%wide.region_1.5_spmd.clone.sunk | while | flops 34410000 | bytes 2141005 | solution.py:249
  35.6 0.8 maximum_bitcast_fusion
  36.5 33.0 %all-gather.13.cloned.1.call-done = f32[4,516,256]{2,1,0:T(8,128)} async-done(((f32[1,516,256]{2,1,0:T(8,128)}), f32[4,516,256]{2,1,0:T(8,128)}) %all-gather.13.cloned.1.call-update) | async-done | bytes 2113552 | tf_op jit(solution)/shard_map/all_gather | solution.py:30
  69.5 0.8 fusion.119
  72.3 2.0 %fusion.50 = f32[512,256]{1,0:T(8,128)S(1)} fusion(f32[512]{0:T(512)S(1)} %broadcast_bitcast_fusion.24, f32[512]{0:T(512)S(1)} %broadcast_bitcast_fusion.25, f32[512]{0:T(512)S(1)} %broadcast_bitcast_fusion.26, f32[512]{0:T(512)S(1)} %broadcast_bitcast_fusion.27, f32[512]{0:T(512)S(1)} %broadcast_bitcast_fusion.28, f32[512]{0:T(512)S(1)} %broadcast_bitcast_fusion.29, ...), kind=kLoop, calls=%fused_computation.111 | loop fusion | flops 1441792 | bytes 2637824 | tf_op jit(solution)/shard_map/add | solution.py:159
  74.3 0.8 fusion.68
  75.0 0.8 maximum_bitcast_fusion.1
  76.0 31.2 %all-gather.15.cloned.1.call-done = f32[4,516,256]{2,1,0:T(8,128)} async-done(((f32[1,516,256]{2,1,0:T(8,128)}), f32[4,516,256]{2,1,0:T(8,128)}) %all-gather.15.cloned.1.call-update) | async-done | bytes 2113552 | tf_op jit(solution)/shard_map/all_gather | solution.py:30
  107.2 0.8 fusion.117
  110.0 2.0 %fusion.43 = f32[512,256]{1,0:T(8,128)S(1)} fusion(f32[512]{0:T(512)S(1)} %broadcast_bitcast_fusion.8, f32[512]{0:T(512)S(1)} %broadcast_bitcast_fusion.9, f32[512]{0:T(512)S(1)} %broadcast_bitcast_fusion.10, f32[512]{0:T(512)S(1)} %broadcast_bitcast_fusion.11, f32[512]{0:T(512)S(1)} %broadcast_bitcast_fusion.12, f32[512]{0:T(512)S(1)} %broadcast_bitcast_fusion.13, ...), kind=kLoop, calls=%fused_computation.100 | loop fusion | flops 1441792 | bytes 2637824 | tf_op jit(solution)/shard_map/add | solution.py:159
  111.9 0.8 fusion.61
  112.7 0.8 maximum_bitcast_fusion.2
  114.3 0.5 multiply_convert_fusion.1
  114.9 0.8 fusion.114
  115.7 2.7 %fusion.120 = (f32[1,512,256]{2,1,0:T(8,128)S(1)}, f32[1,512,256]{2,1,0:T(8,128)}, f32[1,512,256]{2,1,0:T(8,128)}, f32[1,512,256]{2,1,0:T(8,128)}) fusion(f32[4,516,256]{2,1,0:T(8,128)} %all-gather.13.cloned.1.call-done), kind=kLoop, calls=%fused_computation.364 | loop fusion | bytes 4194304 | tf_op jit(solution)/shard_map/slice | solution.py:48
  118.4 0.7 fusion.113
  119.3 2.9 %fusion.118 = (f32[1,512,256]{2,1,0:T(8,128)}, f32[1,512,256]{2,1,0:T(8,128)}, f32[1,512,256]{2,1,0:T(8,128)}, f32[1,512,256]{2,1,0:T(8,128)}) fusion(f32[4,516,256]{2,1,0:T(8,128)} %all-gather.15.cloned.1.call-done), kind=kLoop, calls=%fused_computation.362 | loop fusion | bytes 4194304 | tf_op jit(solution)/shard_map/slice | solution.py:48
  122.1 22.8 %all-gather.17.cloned.1.call-done = f32[4,516,256]{2,1,0:T(8,128)} async-done(((f32[1,516,256]{2,1,0:T(8,128)}), f32[4,516,256]{2,1,0:T(8,128)}) %all-gather.17.cloned.1.call-update) | async-done | bytes 2113552 | tf_op jit(solution)/shard_map/all_gather | solution.py:30
  145.0 0.8 fusion.115
  145.8 0.8 fusion.112
  147.0 1.8 fusion.116
  149.5 1.6 multiply_add_fusion.1
  151.1 10.9 %while.35 = (s32[]{:T(128)}, f32[4,128,256]{2,1,0:T(8,128)S(1)}, f32[4,128]{1,0:T(4,128)S(1)}, f32[4]{0:T(128)S(1)}, f32[3,4,128,256]{3,2,1,0:T(8,128)}, /*index...) while((s32[]{:T(128)}, f32[4,128,256]{2,1,0:T(8,128)S(1)}, ...), condition=%wide.region_13.14_spmd, body=%wide.region_7.13_spmd.sunk | while | flops 119297032 | bytes 5372773 | solution.py:251
  152.9 1.1 fusion.169
  156.6 1.1 fusion.169
  160.2 1.1 fusion.169
  162.0 2.1 %multiply_reduce_fusion = f32[3,128,4]{1,2,0:T(4,128)S(1)} fusion(f32[3,128,4]{1,2,0:T(4,128)S(1)} %get-tuple-element.393, f32[3,4,128,256]{3,2,1,0:T(8,128)} %get-tuple-element.116), kind=kLoop, calls=%fused_computation.71 | loop fusion | flops 1178112 | bytes 1585152 | tf_op jit(solution)/shard_map/reduce_sum | solution.py:254
  164.3 0.5 mul.1186
  164.8 1.6 copy.194
  166.5 0.5 div.42
  167.3 1.0 copy-done.5
  168.4 1.0 copy.155
  169.8 1.1 copy-done.4
  171.3 2.2 %multiply_convert_fusion = bf16[384,1024]{1,0:T(8,128)(2,1)S(1)} fusion(f32[384,1024]{1,0:T(8,128)S(1)} %bitcast.724, f32[384,1024]{1,0:T(8,128)S(1)} %bitcast.726, f32[384,1024]{1,0:T(8,128)S(1)} %bitcast.725, bf16[384,2048]{1,0:T(8,128)(2,1)S(1)} %bitcast.703, bf16[2048,1024]{1,0:T(8,128)(2,1)S(1)} %copy-done.21, f32[1024]{0:T(1024)S(1)} %dynamic-slice-done), kind=kOutput, calls=%fused_computation.70 | convolution fusion | flops 1614544896 | bytes 11276288 | tf_op jit(solution)/shard_map/dot_general | solution.py:209
  173.5 4.8 %all_to_all.25 = bf16[2,192,1024]{2,1,0:T(8,128)(2,1)S(1)} all-to-all(bf16[2,192,1024]{2,1,0:T(8,128)(2,1)S(1)} %bitcast.727), channel_id=1, replica_groups=mesh['sp_0'=4,'sp_1'=4,'sp_2'=4,'tp'=2] {'tp'}, dimensions={0} | all-to-all | bytes 1572864 | tf_op jit(solution)/shard_map/all_to_all | solution.py:264
  178.4 6.2 %convolution_convert_fusion = bf16[192,2048]{1,0:T(8,128)(2,1)} fusion(bf16[192,2048]{1,0:T(8,128)(2,1)S(1)} %bitcast.728, bf16[2048,2048]{1,0:T(8,128)(2,1)} %all-gather.11.cloned.1.call-done), kind=kOutput, calls=%fused_computation.64 | convolution fusion | flops 1611005952 | bytes 9961472 | tf_op jit(solution)/shard_map/dot_general | solution.py:266
  (272 shorter events, 19.3 us)
Async XLA Ops:
  6.5 9.1 %copy-start = (bf16[2048,512]{1,0:T(8,128)(2,1)S(1)}, bf16[2048,512]{1,0:T(8,128)(2,1)}, u32[]{:S(2)}) copy-start(bf16[2048,512]{1,0:T(8,128)(2,1)} %param.20) | copy-start | bytes 6291460
  6.5 63.0 %all-gather.13.cloned.1.call-start = ((), (), s32[]{:S(2)}) async-start(), calls=%async_computation.3 | async-start | bytes 2662400 | tf_op jit(solution)/shard_map/all_gather | solution.py:30
  15.7 1.2 copy-start.2
  15.7 2.2 %copy-start.22 = (bf16[2048,512]{1,0:T(8,128)(2,1)S(1)}, bf16[2048,512]{1,0:T(8,128)(2,1)}, u32[]{:S(2)}) copy-start(bf16[2048,512]{1,0:T(8,128)(2,1)} %param.19) | copy-start | bytes 6291460
  17.8 1.0 copy-start.14
  17.8 4.3 %copy-start.20 = (f32[2,3,4]{2,0,1:T(2,128)S(1)}, f32[2,3,4]{2,0,1:T(2,128)}, u32[]{:S(2)}) copy-start(f32[2,3,4]{2,0,1:T(2,128)} %param.27) | copy-start | bytes 292
  18.8 12.5 %collective-permute-start = (bf16[2,3,512]{2,1,0:T(4,128)(2,1)S(1)}, bf16[2,3,512]{2,1,0:T(4,128)(2,1)S(1)}, u32[]{:S(2)}, u32[]{:S(2)}) collective-permute-start(bf16[2,3,512]{2,1,0:T(4,128)(2,1)S(1)} %pad_maximum_fusion), channel_id=1, source_target_pairs={{0,2},{2,4},{4,6},{6,8},{8,10},{10,12},{12,14},{14,16},{16,18},{18... | collective-permute-start | bytes 18440 | tf_op jit(solution)/shard_map/ppermute | solution.py:73
  22.1 5.5 %copy-start.3 = (bf16[2,192,2048]{2,1,0:T(8,128)(2,1)S(1)}, bf16[2,192,2048]{2,1,0:T(8,128)(2,1)}, u32[]{:S(2)}) copy-start(bf16[2,192,2048]{2,1,0:T(8,128)(2,1)} %copy-done.2) | copy-start | bytes 4718596
  22.1 5.5 %copy-start.16 = (bf16[2048,8]{0,1:T(8,128)(2,1)S(1)}, bf16[2048,8]{0,1:T(8,128)(2,1)}, u32[]{:S(2)}) copy-start(bf16[2048,8]{0,1:T(8,128)(2,1)} %param.24) | copy-start | bytes 98308
  27.6 0.8 copy-start.17
  27.6 1.2 copy-start.18
  27.6 1.2 copy-start.19
  29.1 2.2 %copy-start.15 = (bf16[384,512]{1,0:T(8,128)(2,1)S(1)}, bf16[384,512]{1,0:T(8,128)(2,1)}, u32[]{:S(2)}) copy-start(bf16[384,512]{1,0:T(8,128)(2,1)} %copy-done.14) | copy-start | bytes 1179652
  36.5 70.7 %all-gather.15.cloned.1.call-start = ((), (), s32[]{:S(2)}) async-start(), calls=%async_computation.4 | async-start | bytes 2662400 | tf_op jit(solution)/shard_map/all_gather | solution.py:30
  75.9 69.1 %all-gather.17.cloned.1.call-start = ((), (), s32[]{:S(2)}) async-start(), calls=%async_computation.5 | async-start | bytes 2662400 | tf_op jit(solution)/shard_map/all_gather | solution.py:30
  113.6 64.8 %all-gather.11.cloned.1.call-start = ((), (), s32[]{:S(2)}) async-start(), calls=%async_computation.2 | async-start | bytes 12582912 | tf_op jit(solution)/shard_map/all_gather | solution.py:265
  146.9 1.9 copy-start.6
  146.9 1.9 copy-start.7
  146.9 2.0 %copy-start.8 = (f32[1,512,256]{2,1,0:T(8,128)S(1)}, f32[1,512,256]{2,1,0:T(8,128)}, u32[]{:S(2)}) copy-start(f32[1,512,256]{2,1,0:T(8,128)} %get-tuple-element.391) | copy-start | bytes 1572868
  146.9 2.1 %copy-start.9 = (f32[1,512,256]{2,1,0:T(8,128)S(1)}, f32[1,512,256]{2,1,0:T(8,128)}, u32[]{:S(2)}) copy-start(f32[1,512,256]{2,1,0:T(8,128)} %get-tuple-element.382) | copy-start | bytes 1572868
  146.9 2.3 %copy-start.10 = (f32[1,512,256]{2,1,0:T(8,128)S(1)}, f32[1,512,256]{2,1,0:T(8,128)}, u32[]{:S(2)}) copy-start(f32[1,512,256]{2,1,0:T(8,128)} %get-tuple-element.383) | copy-start | bytes 1572868
  146.9 2.4 %copy-start.11 = (f32[1,512,256]{2,1,0:T(8,128)S(1)}, f32[1,512,256]{2,1,0:T(8,128)}, u32[]{:S(2)}) copy-start(f32[1,512,256]{2,1,0:T(8,128)} %get-tuple-element.384) | copy-start | bytes 1572868
  147.0 2.6 %copy-start.12 = (f32[1,512,256]{2,1,0:T(8,128)S(1)}, f32[1,512,256]{2,1,0:T(8,128)}, u32[]{:S(2)}) copy-start(f32[1,512,256]{2,1,0:T(8,128)} %get-tuple-element.385) | copy-start | bytes 1572868
  167.0 1.4 copy-start.5
  167.0 2.8 %copy-start.21 = (bf16[2048,1024]{1,0:T(8,128)(2,1)S(1)}, bf16[2048,1024]{1,0:T(8,128)(2,1)}, u32[]{:S(2)}) copy-start(bf16[2048,1024]{1,0:T(8,128)(2,1)} %param.22) | copy-start | bytes 12582916
  169.4 1.5 copy-start.4
  169.4 1.9 %copy-start.13 = (f32[48,8,4,256]{3,1,2,0:T(8,128)S(1)}, f32[48,8,4,256]{3,1,2,0:T(8,128)}, u32[]{:S(2)}) copy-start(f32[48,8,4,256]{3,1,2,0:T(8,128)} %copy.194) | copy-start | bytes 4718596
  169.4 1.9 dynamic-slice-start
  178.4 6.2 %copy-start.1 = (bf16[2048,512]{1,0:T(8,128)(2,1)S(1)}, bf16[2048,512]{1,0:T(8,128)(2,1)}, u32[]{:S(2)}) copy-start(bf16[2048,512]{1,0:T(8,128)(2,1)} %param.20) | copy-start | bytes 6291460
Sparse Core Ops, SparseCore 0:
  36.6 32.9 all-gather.12
  76.0 31.0 all-gather.14
  113.7 31.2 all-gather.16
  146.5 23.0 all-gather.10
where the time goes:
time: 192 us; the launch traced here: 191 us
  waiting for transfers between devices  87.5 us (46%)
  local copies, waits for them, and re-layouts  30.1 us (16%)
  matrix products  24.2 us (13%)
  other arithmetic  20.9 us (11%)
  between operations  13.9 us (7%)
  blocking collectives  10.8 us (6%)
  starting transfers between devices  3.54 us (2%)
    all_gather x3, waiting for transfers between devices, gathered_once(): both, at, found = (lax.all_gather(jnp.concatenate(lines), axis), 0, {})  87.1 us
    slice x8, local copies, waits for them, and re-layouts, carried_in(): running = combine(running, jax.tree.map(lambda part: part[k], pieces))  9.72 us
    unnamed x74, local copies, waits for them, and re-layouts  8.25 us
    dot_general x1, matrix products, body(): jnp.dot(by_token, full_weight, preferred_element_type=jnp.float32)  6.21 us
    all_to_all x1, blocking collectives, sent_to_all(): return lax.all_to_all(copies, axis, split_axis=0, concat_axis=0, tiled=True)  6.01 us
    add x3, other arithmetic, join_states(): scale_one[:, None, None] * states_one  5.5 us
    dot_general x1, matrix products, body(): jnp.dot(gathered, w_value, preferred_element_type=jnp.float32)  5.45 us
    all_to_all x1, blocking collectives, body(): lax.all_to_all(hidden, 'tp', split_axis=0, concat_axis=1, tiled=True)  4.76 us
  transfers between devices with their start and end apart: 5, of which 3 were waited for; matrix products, arithmetic and copies ran while one was open for 22% of the time, Pallas kernels for 0%

commit v1 on v0

v1 whole, which is shorter than its diff:
```python
import functools

import jax
import jax.numpy as jnp
from jax import lax
from jax.experimental import pallas as pl
from jax.experimental.pallas import tpu as pltpu
from jax.sharding import Mesh
from jax.sharding import PartitionSpec as P

SPAN = 128
SP = ("sp_0", "sp_1", "sp_2")
SP_TP = ("sp_0", "sp_1", "sp_2", "tp")
EPS = 1e-06
EMPTY = -1e30
TAIL = 16
HEADS = 4
DQK = 128
DV = 256
WIDTH = DV + 128
BLOCKS = 3
ROWS = BLOCKS * SPAN
HALF = ROWS // 2
HIGHEST = lax.Precision.HIGHEST
BF = jnp.bfloat16
F32 = jnp.float32
MIB = 1 << 20


def in_vmem():
    return pl.BlockSpec(memory_space=pltpu.VMEM)


def in_hbm():
    return pl.BlockSpec(memory_space=pl.ANY)


def call(kernel, outs, ins, scratch=(), flops=0, limit=40):
    return pl.pallas_call(
        kernel,
        out_shape=outs,
        in_specs=ins,
        out_specs=jax.tree.map(lambda _: in_vmem(), outs),
        scratch_shapes=list(scratch),
        cost_estimate=pl.CostEstimate(flops=flops, transcendentals=0, bytes_accessed=1 << 20),
        compiler_params=pltpu.CompilerParams(vmem_limit_bytes=limit * MIB),
    )


def thirds(x):
    hi = x.astype(BF).astype(F32)
    rest = x - hi
    mid = rest.astype(BF).astype(F32)
    return hi, mid, (rest - mid).astype(BF).astype(F32)


def lane_of(shape):
    return lax.broadcasted_iota(jnp.int32, shape, len(shape) - 1)


def mixed_rows(pre_ref, taps, lanes, first, rows):
    acc = None
    for j in range(4):
        term = taps[j : j + 1, lanes] * pre_ref[pl.ds(first + TAIL - 3 + j, rows), lanes]
        acc = term if acc is None else acc + term
    return acc * (1.0 / (1.0 + jnp.exp(-acc)))


def summary_kernel(own_ref, oth_ref, one_ref, two_ref, gain_ref, wk_hbm, wv_hbm, wg_ref, taps_ref, offs_ref,
                   key_ref, value_ref, logs_ref, piece_ref, rows_ref, wk_ref, wv_ref, pre_ref, sems):
    wide = HEADS * DV // 2
    copies = [pltpu.make_async_copy(wk_hbm, wk_ref, sems.at[0])]
    for c in range(2):
        cols = pl.ds(c * wide, wide)
        copies.append(pltpu.make_async_copy(wv_hbm.at[:, cols], wv_ref.at[:, cols], sems.at[1 + c]))
    for copy in copies:
        copy.start()
    tp = lax.axis_index("tp")
    gain = gain_ref[...]

    def normalized(x):
        x = x.astype(F32)
        scale = lax.rsqrt(jnp.mean(x * x, axis=-1, keepdims=True) + EPS)
        return (x * scale * gain).astype(BF)

    rows_ref[0:TAIL, :] = normalized(one_ref[...] + two_ref[...])
    for ref, at in ((own_ref, tp), (oth_ref, 1 - tp)):
        for part in range(HALF // 48):
            to = pl.multiple_of(TAIL + at * HALF + part * 48, 16)
            rows_ref[pl.ds(to, 48), :] = normalized(ref[part * 48 : part * 48 + 48, :])
    own = pl.ds(TAIL, ROWS)
    gates = jnp.dot(rows_ref[own, :], wg_ref[...], preferred_element_type=F32)
    copies[0].wait()
    pre_ref[...] = jnp.dot(rows_ref[...], wk_ref[...], preferred_element_type=F32).astype(BF).astype(F32)

    lane = lane_of((SPAN, 128))
    tri = (lax.broadcasted_iota(jnp.int32, (SPAN, SPAN), 0) >= lax.broadcasted_iota(jnp.int32, (SPAN, SPAN), 1)).astype(F32)
    gate, inside, totals = [], [], []
    for b in range(BLOCKS):
        g = gates[b * SPAN : (b + 1) * SPAN] + offs_ref[b : b + 1, :]
        soft = jnp.minimum(g, 0.0) - jnp.log1p(jnp.exp(-jnp.abs(g)))
        total = jnp.dot(tri, soft, precision=HIGHEST, preferred_element_type=F32)
        logs_ref[b * SPAN : (b + 1) * SPAN, :] = jnp.where(lane < HEADS, g, total)
        total = pltpu.roll(total, 128 - HEADS, 1)
        gate.append(g)
        inside.append(total)
        totals.append(total[SPAN - 1 : SPAN, :])
    write, level = [], None
    later = jnp.zeros_like(totals[0])
    for b in reversed(range(BLOCKS)):
        w = (totals[b] - inside[b]) + later + gate[b]
        later = later + totals[b]
        write.insert(0, w)
        top = jnp.max(w, axis=0, keepdims=True)
        level = top if level is None else jnp.maximum(level, top)
    weight = [jnp.exp(w - level) for w in write]
    numbers = thirds(later) + thirds(level)

    taps = taps_ref[:, pl.ds(pl.multiple_of(tp * (HEADS * DQK), 128), HEADS * DQK)].astype(F32)
    for h in range(HEADS):
        lanes = slice(h * DQK, (h + 1) * DQK)
        for b in range(BLOCKS):
            rows = slice(b * SPAN, (b + 1) * SPAN)
            key_ref[rows, lanes] = (mixed_rows(pre_ref, taps, lanes, b * SPAN, SPAN) * DQK**-0.5).astype(BF)
    for c in range(2):
        copies[1 + c].wait()
        cols = slice(c * wide, (c + 1) * wide)
        value_ref[:, cols] = jnp.dot(rows_ref[own, :], wv_ref[:, cols], preferred_element_type=F32).astype(BF)
    ones = jnp.ones((ROWS, 128), BF)
    dims = (((0,), (0,)), ((), ()))
    for h in range(HEADS):
        lanes = slice(h * DQK, (h + 1) * DQK)
        weighted = jnp.concatenate(
            [
                (key_ref[b * SPAN : (b + 1) * SPAN, lanes].astype(F32) * weight[b][:, h : h + 1]).astype(BF)
                for b in range(BLOCKS)
            ],
            axis=0,
        )
        memory = lax.dot_general(weighted, value_ref[:, h * DV : (h + 1) * DV], dims, preferred_element_type=F32)
        extra = lax.dot_general(weighted, ones, dims, preferred_element_type=F32)
        for n, number in enumerate(numbers):
            extra = jnp.where(lane == n + 1, number[:, h : h + 1], extra)
        out = slice(h * DQK, (h + 1) * DQK)
        piece_ref[out, :DV] = memory.astype(BF)
        piece_ref[out, DV:] = extra.astype(BF)


def prefix_kernel(piece_ref, out_ref, wide_ref, done_ref):
    count = piece_ref.shape[0]
    wide_ref[...] = piece_ref[...].astype(F32)
    extra = wide_ref[:, 0, DV:]
    lane = lane_of((count, 128))

    def number(first):
        return jnp.sum(jnp.where((lane >= first) & (lane < first + 3), extra, 0.0), axis=1, keepdims=True)

    forget, level = number(1), number(4)
    down = lax.broadcasted_iota(jnp.int32, (count, count), 0)
    over = lax.broadcasted_iota(jnp.int32, (count, count), 1)
    steps = jnp.where(down > over, forget, jnp.where(down == over, level, 0.0))
    earlier = over < down
    logs = jnp.dot(earlier.astype(F32), steps, precision=HIGHEST, preferred_element_type=F32)
    logs = jnp.where(earlier, logs, EMPTY)
    top = jnp.max(logs, axis=1, keepdims=True)
    weight = jnp.where(earlier, jnp.exp(logs - top), 0.0)
    high = weight.astype(BF)
    low = (weight - high.astype(F32)).astype(BF)
    marks = thirds(top)
    lane = lane_of((count, WIDTH))
    for r in range(8):
        part = wide_ref[:, r, :].astype(BF)
        state = jnp.dot(high, part, preferred_element_type=F32) + jnp.dot(low, part, preferred_element_type=F32)
        for n, mark in enumerate(marks):
            state = jnp.where(lane == DV + 1 + n, mark, state)
        done_ref[:, r, :] = state
    out_ref[...] = done_ref[...].astype(BF)


def query_kernel(rows_ref, wq_hbm, wo_hbm, taps_ref, gain_ref, query_ref, ogate_ref, wq_ref, wo_ref, pre_ref, sems):
    wide = HEADS * DV // 2
    copies = [pltpu.make_async_copy(wq_hbm, wq_ref, sems.at[0])]
    for c in range(2):
        cols = pl.ds(c * wide, wide)
        copies.append(pltpu.make_async_copy(wo_hbm.at[:, cols], wo_ref.at[:, cols], sems.at[1 + c]))
    for copy in copies:
        copy.start()
    tp = lax.axis_index("tp")
    taps = taps_ref[:, pl.ds(pl.multiple_of(tp * (HEADS * DQK), 128), HEADS * DQK)].astype(F32)
    gain = gain_ref[:, pl.ds(pl.multiple_of(tp * (HEADS * DV), 128), HEADS * DV)]
    copies[0].wait()
    pre_ref[...] = jnp.dot(rows_ref[...], wq_ref[...], preferred_element_type=F32).astype(BF).astype(F32)
    for h in range(HEADS):
        lanes = slice(h * DQK, (h + 1) * DQK)
        for b in range(BLOCKS):
            rows = slice(b * SPAN, (b + 1) * SPAN)
            query_ref[rows, lanes] = mixed_rows(pre_ref, taps, lanes, b * SPAN, SPAN).astype(BF)
    for c in range(2):
        copies[1 + c].wait()
        cols = slice(c * wide, (c + 1) * wide)
        pre = jnp.dot(rows_ref[pl.ds(TAIL, ROWS), :], wo_ref[:, cols], preferred_element_type=F32).astype(BF).astype(F32)
        ogate_ref[:, cols] = gain[:, cols] / (1.0 + jnp.exp(-pre))


def local_kernel(query_ref, key_ref, value_ref, logs_ref, numer_ref, stats_ref):
    lane = lane_of((SPAN, 128))
    cols = [logs_ref[b * SPAN : (b + 1) * SPAN, :] for b in range(BLOCKS)]
    flat = [c.T for c in cols]
    ends = [c[SPAN - 1 : SPAN, :] for c in cols]
    causal = lax.broadcasted_iota(jnp.int32, (SPAN, SPAN), 0) >= lax.broadcasted_iota(jnp.int32, (SPAN, SPAN), 1)
    stats = []
    before = jnp.zeros_like(ends[0])
    for b in range(BLOCKS):
        carried = pltpu.roll(cols[b] + before, HEADS, 1)
        before = before + ends[b]
        stats.append(jnp.where((lane >= 2 * HEADS) & (lane < 3 * HEADS), carried, 0.0))
    nt = (((1,), (1,)), ((), ()))
    for h in range(HEADS):
        head = slice(h * DQK, (h + 1) * DQK)
        for t in range(BLOCKS):
            rows = slice(t * SPAN, (t + 1) * SPAN)
            seen = (t + 1) * SPAN
            now = cols[t][:, HEADS + h : HEADS + h + 1]
            logs = []
            for s in range(t + 1):
                gate = flat[s][h : h + 1, :]
                past = flat[s][HEADS + h : HEADS + h + 1, :]
                if s == t:
                    logs.append(jnp.where(causal, (now - past) + gate, EMPTY))
                else:
                    rest = ends[s][:, HEADS + h : HEADS + h + 1] - past
                    for c in range(s + 1, t):
                        rest = rest + ends[c][:, HEADS + h : HEADS + h + 1]
                    logs.append(now + (rest + gate))
            top = None
            for x in logs:
                peak = jnp.max(x, axis=1, keepdims=True)
                top = peak if top is None else jnp.maximum(top, peak)
            weight = jnp.concatenate([jnp.exp(x - top) for x in logs], axis=1)
            scores = (
                lax.dot_general(query_ref[rows, head], key_ref[:seen, head], nt, preferred_element_type=F32) * weight
            )
            denom = jnp.sum(scores, axis=1, keepdims=True)
            numer_ref[rows, h * DV : (h + 1) * DV] = jnp.dot(
                scores.astype(BF), value_ref[:seen, h * DV : (h + 1) * DV], preferred_element_type=F32
            )
            stats[t] = jnp.where(lane == h, denom, jnp.where(lane == HEADS + h, top, stats[t]))
    for t in range(BLOCKS):
        stats_ref[t * SPAN : (t + 1) * SPAN, :] = stats[t]


def hidden_rows(first, query_ref, ogate_ref, state_ref, numer_ref, stats_ref, hidden_ref):
    rows = pl.ds(pl.multiple_of(first, 16), HALF)
    lane = lane_of((HALF, 128))
    stats = stats_ref[rows, :]
    place = lane_of((DQK, 128))
    norms, level = [], jnp.zeros((1, 128), F32)
    for h in range(HEADS):
        extra = state_ref[h * DQK : (h + 1) * DQK, DV:].astype(F32)
        norms.append(jnp.where(place == h, extra[:, 0:1], 0.0).astype(BF))
        mark = extra[0:1, 1:2] + extra[0:1, 2:3] + extra[0:1, 3:4]
        level = jnp.where(lane_of((1, 128)) == h, mark, level)
    norms = jnp.concatenate(norms, axis=0)
    query = query_ref[rows, :]
    read_norm = jnp.dot(query, norms, preferred_element_type=F32)
    top = pltpu.roll(stats, 128 - HEADS, 1)
    carried = pltpu.roll(stats, 128 - 2 * HEADS, 1) + level
    peak = jnp.maximum(carried, top)
    one = jnp.exp(carried - peak)
    two = jnp.exp(top - peak)
    denom = one * read_norm + two * stats
    denom = jnp.maximum(jnp.abs(denom), jnp.exp(-peak))
    one = one / denom
    two = two / denom
    for h in range(HEADS):
        wide = slice(h * DV, (h + 1) * DV)
        read = jnp.dot(
            query[:, h * DQK : (h + 1) * DQK], state_ref[h * DQK : (h + 1) * DQK, :DV], preferred_element_type=F32
        )
        cell = one[:, h : h + 1] * read + two[:, h : h + 1] * numer_ref[rows, wide]
        scale = lax.rsqrt(jnp.mean(cell * cell, axis=-1, keepdims=True) + EPS)
        hidden_ref[:, wide] = (cell * scale * ogate_ref[rows, wide]).astype(BF)


def sent_kernel(query_ref, ogate_ref, state_ref, numer_ref, stats_ref, wout_ref, out_ref, hidden_ref):
    first = (1 - lax.axis_index("tp")) * HALF
    hidden_rows(first, query_ref, ogate_ref, state_ref, numer_ref, stats_ref, hidden_ref)
    out_ref[...] = jnp.dot(hidden_ref[...], wout_ref[...], preferred_element_type=F32).astype(BF)


def kept_kernel(query_ref, ogate_ref, state_ref, numer_ref, stats_ref, wout_ref, out_ref, hidden_ref):
    first = lax.axis_index("tp") * HALF
    hidden_rows(first, query_ref, ogate_ref, state_ref, numer_ref, stats_ref, hidden_ref)
    out_ref[...] = jnp.dot(hidden_ref[...], wout_ref[...], preferred_element_type=F32)


def body(
    tokens, norm_gain, w_query, w_key, w_value, w_ogate, w_igate, w_fgate, conv_query, conv_key, gate_offset, head_gain, w_out
):
    tp = lax.axis_index("tp")
    width = tokens.shape[1]
    first = tp * HEADS
    stretches = lax.axis_size(SP)
    shape = jax.ShapeDtypeStruct
    other = lax.ppermute(tokens, "tp", [(0, 1), (1, 0)])
    last = tokens[HALF - TAIL :]
    to_second = lax.ppermute(last, SP_TP, [(2 * i + 1, 2 * i + 3) for i in range(stretches - 1)])
    to_first = lax.ppermute(last, SP_TP, [(2 * i + 1, 2 * i + 2) for i in range(stretches - 1)])
    w_gates = jnp.concatenate(
        [lax.dynamic_slice_in_dim(w_igate, first, HEADS, 1), lax.dynamic_slice_in_dim(w_fgate, first, HEADS, 1)], axis=1
    )
    w_gates = jnp.pad(w_gates, ((0, 0), (0, 128 - 2 * HEADS)))
    offsets = jnp.concatenate([gate_offset[0], gate_offset[1]], axis=1)
    offsets = jnp.pad(offsets, ((0, 0), (0, 128 - 2 * HEADS)))
    gain = norm_gain.reshape(1, -1)
    head_gain = head_gain.reshape(1, -1)
    v, m = in_vmem(), in_hbm()
    key, value, logs, pieces, rows = call(
        summary_kernel,
        (
            shape((ROWS, HEADS * DQK), BF),
            shape((ROWS, HEADS * DV), BF),
            shape((ROWS, 128), F32),
            shape((HEADS * DQK, WIDTH), BF),
            shape((TAIL + ROWS, width), BF),
        ),
        [v, v, v, v, v, m, m, v, v, v],
        [
            pltpu.VMEM((width, HEADS * DQK), BF),
            pltpu.VMEM((width, HEADS * DV), BF),
            pltpu.VMEM((TAIL + ROWS, HEADS * DQK), F32),
            pltpu.SemaphoreType.DMA((3,)),
        ],
        flops=3_000_000_000,
    )(tokens, other, to_first, to_second, gain, w_key, w_value, w_gates, conv_key, offsets)
    pieces = pieces.reshape(stretches, 8, WIDTH)
    pieces = lax.all_to_all(pieces, SP, 0, 0, tiled=True)
    query, ogate = call(
        query_kernel,
        (shape((ROWS, HEADS * DQK), BF), shape((ROWS, HEADS * DV), F32)),
        [v, m, m, v, v],
        [
            pltpu.VMEM((width, HEADS * DQK), BF),
            pltpu.VMEM((width, HEADS * DV), BF),
            pltpu.VMEM((TAIL + ROWS, HEADS * DQK), F32),
            pltpu.SemaphoreType.DMA((3,)),
        ],
        flops=3_000_000_000,
    )(rows, w_query, w_ogate, conv_query, head_gain)
    state = call(
        prefix_kernel,
        shape((stretches, 8, WIDTH), BF),
        [v],
        [pltpu.VMEM((stretches, 8, WIDTH), F32), pltpu.VMEM((stretches, 8, WIDTH), F32)],
        flops=100_000_000,
    )(pieces)
    state = lax.all_to_all(state, SP, 0, 0, tiled=True).reshape(HEADS * DQK, WIDTH)
    numer, stats = call(
        local_kernel,
        (shape((ROWS, HEADS * DV), F32), shape((ROWS, 128), F32)),
        [v, v, v, v],
        flops=1_000_000_000,
    )(query, key, value, logs)
    hidden = pltpu.VMEM((HALF, HEADS * DV), BF)
    sent = call(sent_kernel, shape((HALF, width), BF), [v] * 6, [hidden], flops=1_000_000_000)(
        query, ogate, state, numer, stats, w_out
    )
    got = lax.ppermute(sent, "tp", [(0, 1), (1, 0)])
    kept = call(kept_kernel, shape((HALF, width), F32), [v] * 6, [hidden], flops=1_000_000_000)(
        query, ogate, state, numer, stats, w_out
    )
    return (kept + got.astype(F32)).astype(BF)


def solution(mesh):
    split = Mesh(mesh.devices.reshape(4, 4, 4, mesh.shape["tp"]), ("sp_0", "sp_1", "sp_2", "tp"))
    placed = (
        P(SP_TP, None),
        P(),
        P(None, "tp"),
        P(None, "tp"),
        P(None, "tp"),
        P(None, "tp"),
        P(),
        P(),
        P(),
        P(),
        P(None, SP, "tp"),
        P(),
        P("tp", None),
    )
    return jax.shard_map(
        body, mesh=split, in_specs=placed, out_specs=P(SP_TP, None), check_vma=False
    )
```

time: 192 us -> 75.9 us (0.40)
  waiting for transfers between devices: 87.5 us -> 1.15 us
  matrix products: 24.2 us -> 0 us
  other arithmetic: 20.9 us -> 1.17 us
  Pallas kernels: 0 us -> 19.4 us
  between operations: 13.9 us -> 0.24 us
  blocking collectives: 10.8 us -> 21.9 us
  local copies, waits for them, and re-layouts: 30.1 us -> 19.3 us
  starting transfers between devices: 3.54 us -> 12.1 us
    all_gather x4 -> x0, waiting for transfers between devices: 87.1 us -> none  [the longest x3 87.1 us: gathered_once(): both, at, found = (lax.all_gather(jnp.concatenate(lines), axis), 0, {})]
    dot_general x25 -> x0, matrix products: 24.2 us -> none  [the longest x1 6.21 us: body(): jnp.dot(by_token, full_weight, preferred_element_type=jnp.float32)]
    pallas_call x0 -> x6, Pallas kernels: none -> 19.4 us  [the longest x1 6.48 us: body(): call(summary_kernel, (shape((ROWS, HEADS * DQK), BF), shape((ROWS, HEADS...]
    slice x15 -> x2, local copies, waits for them, and re-layouts: 12.8 us -> 0.92 us  [the longest x1 0.92 us: body(): last = tokens[HALF - TAIL:]]
    all_to_all x2 -> x1, blocking collectives: 10.8 us -> 21.9 us  [body(): pieces = lax.all_to_all(pieces, SP, 0, 0, tiled=True)]
    unnamed x74 -> x47, local copies, waits for them, and re-layouts: 8.25 us -> 17.2 us
    add x13 -> x0, other arithmetic: 7.65 us -> none  [the longest x3 5.5 us: join_states(): scale_one[:, None, None] * states_one]
    all_to_all x0 -> x1, starting transfers between devices: none -> 4.81 us  [body(): lax.all_to_all(state, SP, 0, 0, tiled=True).reshape(HEADS * DQK, WIDTH)]
  transfers between devices with their start and end apart: 5 -> 5, of which waited for: 3 -> 1; matrix products, arithmetic and copies ran while one was open for 22% -> 2% of each run, Pallas kernels for 0% -> 11%
where the time goes in v1:
time: 75.9 us; the launch traced here: 75.2 us
  blocking collectives  21.9 us (29%)
  Pallas kernels  19.4 us (26%)
  local copies, waits for them, and re-layouts  19.3 us (25%)
  starting transfers between devices  12.1 us (16%)
  other arithmetic  1.17 us (2%)
  waiting for transfers between devices  1.15 us (2%)
    all_to_all x1, blocking collectives, body(): pieces = lax.all_to_all(pieces, SP, 0, 0, tiled=True)  21.9 us
    unnamed x47, local copies, waits for them, and re-layouts  17.2 us
    pallas_call x1, Pallas kernels, body(): call(summary_kernel, (shape((ROWS, HEADS * DQK), BF), shape((ROWS, HEADS...  6.48 us
    all_to_all x1, starting transfers between devices, body(): lax.all_to_all(state, SP, 0, 0, tiled=True).reshape(HEADS * DQK, WIDTH)  4.81 us
    pallas_call x1, Pallas kernels, body(): call(query_kernel, (shape((ROWS, HEADS * DQK), BF), shape((ROWS, HEADS *...  4.68 us
    ppermute x1, starting transfers between devices, body(): lax.ppermute(last, SP_TP, [(2 * i + 1, 2 * i + 3) for i in range(stretche...  3.92 us
    pallas_call x1, Pallas kernels, body(): call(prefix_kernel, shape((stretches, 8, WIDTH), BF), [v], [pltpu.VMEM((s...  2.22 us
    pallas_call x1, Pallas kernels, body(): call(sent_kernel, shape((HALF, width), BF), [v] * 6, [hidden], flops=1000...  2.03 us
  transfers between devices with their start and end apart: 5, of which 1 were waited for; matrix products, arithmetic and copies ran while one was open for 2% of the time, Pallas kernels for 11%

profile of v1, /device:TPU:1, one launch (start us, length us, event | category | flops | bytes accessed | tf_op | source)
XLA Modules:
  0.0 75.2 jit_solution(17713412667762345757)
XLA Ops:
  0.0 0.0 copy-start.10
  0.0 0.9 %slice.9 = bf16[16,2048]{1,0:T(8,128)(2,1)S(1)} slice(bf16[192,2048]{1,0:T(8,128)(2,1)} %own_ref.1), slice={[176:192], [0:2048]} | slice | bytes 131072 | tf_op jit(solution)/shard_map/slice | solution.py:306
  0.9 3.9 %collective-permute-start.2 = (bf16[16,2048]{1,0:T(8,128)(2,1)S(1)}, bf16[16,2048]{1,0:T(8,128)(2,1)S(1)}, u32[]{:S(2)}, u32[]{:S(2)}) collective-permute-start(bf16[16,2048]{1,0:T(8,128)(2,1)S(1)} %slice.9), channel_id=1, source_target_pairs={{1,3},{3,5},{5,7},{7,9},{9,11},{11,13},{13,15},{15,17},{17,19},{19... | collective-permute-start | bytes 196616 | tf_op jit(solution)/shard_map/ppermute | solution.py:307
  4.9 1.3 %collective-permute-start.1 = (bf16[16,2048]{1,0:T(8,128)(2,1)S(1)}, bf16[16,2048]{1,0:T(8,128)(2,1)S(1)}, u32[]{:S(2)}, u32[]{:S(2)}) collective-permute-start(bf16[16,2048]{1,0:T(8,128)(2,1)S(1)} %slice.9), channel_id=1, source_target_pairs={{1,2},{3,4},{5,6},{7,8},{9,10},{11,12},{13,14},{15,16},{17,18},{19... | collective-permute-start | bytes 196616 | tf_op jit(solution)/shard_map/ppermute | solution.py:308
  6.2 0.1 collective-permute-start
  6.3 0.8 %constant_dynamic-slice_fusion = (bf16[2048,4]{0,1:T(4,128)(2,1)S(1)}, bf16[2048,4]{0,1:T(4,128)(2,1)S(1)}) fusion(bf16[2048,8]{0,1:T(8,128)(2,1)} %param.20, s32[]{:T(128)S(6)} %select_n.4, bf16[2048,8]{0,1:T(8,128)(2,1)} %param.19), kind=kLoop, calls=%fused_computation.6 | loop fusion | bytes 65540 | tf_op jit(solution)/shard_map/dynamic_slice | solution.py:310
  7.1 0.3 copy.18
  7.4 0.1 pad.8.wg_ref
  7.5 0.0 copy-done.22
  7.5 0.1 select_maximum_fusion.offs_ref
  7.6 0.0 collective-permute-done.2.two_ref
  7.6 0.0 collective-permute-done.1.one_ref
  7.6 1.1 %collective-permute-done.oth_ref = bf16[192,2048]{1,0:T(8,128)(2,1)S(1)} collective-permute-done((bf16[192,2048]{1,0:T(8,128)(2,1)}, bf16[192,2048]{1,0:T(8,128)(2,1)S(1)}, u32[]{:S(2)}, u32[]{:S(2)}) %collective-permute-start) | collective-permute-done | bytes 786464 | tf_op jit(solution)/shard_map/ppermute | solution.py:305
  8.7 0.0 copy-done.5
  8.7 0.0 copy-done.11
  8.8 0.0 copy-done.10
  8.8 0.0 copy-start.6
  8.8 2.2 %copy-done.6 = bf16[2048,1024]{1,0:T(8,128)(2,1)S(1)} copy-done((bf16[2048,1024]{1,0:T(8,128)(2,1)S(1)}, bf16[2048,1024]{1,0:T(8,128)(2,1)}, u32[]{:S(2)}) %copy-start.6) | copy-done | bytes 4194328
  10.9 1.6 %copy-done.8 = bf16[2048,512]{1,0:T(8,128)(2,1)S(1)} copy-done((bf16[2048,512]{1,0:T(8,128)(2,1)S(1)}, bf16[2048,512]{1,0:T(8,128)(2,1)}, u32[]{:S(2)}) %copy-start.8) | copy-done | bytes 2097176
  12.5 6.5 %shard_map.127 = (bf16[384,512]{1,0:T(8,128)(2,1)S(1)}, bf16[384,1024]{1,0:T(8,128)(2,1)S(1)}, f32[384,128]{1,0:T(8,128)S(1)}, bf16[512,384]{1,0:T(8,128)(2,1)S(1)}, bf16[400,2048]{1,0:T(8,128)(2,1)S(1)}) custom-call(bf16[192,2048]{1,0:T(8,128)(2,1)S(1)} %copy-done.5, bf16[192,2048]{1,0:T(8,128)(2,1)S(1)} %collective-permute-done.oth_ref, ...), custom_call_target="tpu_custom_call" | custom-call | flops 3000000000 | bytes 1048576 | tf_op jit(solution)/shard_map/pallas_call | solution.py:318
  19.0 0.0 copy-start.14
  19.0 1.2 %copy-done.14 = bf16[400,2048]{1,0:T(8,128)(2,1)} copy-done((bf16[400,2048]{1,0:T(8,128)(2,1)}, bf16[400,2048]{1,0:T(8,128)(2,1)S(1)}, u32[]{:S(2)}) %copy-start.14) | copy-done | bytes 1638424
  20.3 0.7 copy-done.18
  21.0 0.7 copy-done.20
  21.7 21.9 %all_to_all.10.piece_ref = bf16[64,8,384]{2,1,0:T(8,128)(2,1)S(1)} all-to-all(bf16[64,8,384]{2,1,0:T(8,128)(2,1)S(1)} %bitcast.10), channel_id=1, replica_groups=mesh['sp_0'=4,'sp_1'=4,'sp_2'=4,'tp'=2] {'sp_0','sp_1','sp_2'}, dimensions={0} | all-to-all | bytes 786432 | tf_op jit(solution)/shard_map/all_to_all | solution.py:337
  43.6 0.0 copy-done.16
  43.6 2.2 %shard_map.129 = bf16[64,8,384]{2,1,0:T(8,128)(2,1)} custom-call(bf16[64,8,384]{2,1,0:T(8,128)(2,1)S(1)} %all_to_all.10.piece_ref), custom_call_target="tpu_custom_call" | custom-call | flops 100000000 | bytes 1048576 | tf_op jit(solution)/shard_map/pallas_call | solution.py:350
  45.8 4.8 %all-to-all-start.1 = ((bf16[64,8,384]{2,1,0:T(8,128)(2,1)}), bf16[64,8,384]{2,1,0:T(8,128)(2,1)S(1)}, u32[]{:S(2)}, u32[]{:S(2)}) async-start(bf16[64,8,384]{2,1,0:T(8,128)(2,1)} %shard_map.129), calls=%async_computation.1 | async-start | bytes 786432 | tf_op jit(solution)/shard_map/all_to_all | solution.py:357
  50.6 0.0 copy-done.12
  50.7 0.0 copy-done.13
  50.7 0.0 copy-start.7
  50.7 2.2 %copy-done.7 = bf16[2048,1024]{1,0:T(8,128)(2,1)S(1)} copy-done((bf16[2048,1024]{1,0:T(8,128)(2,1)S(1)}, bf16[2048,1024]{1,0:T(8,128)(2,1)}, u32[]{:S(2)}) %copy-start.7) | copy-done | bytes 4194328
  52.9 1.6 %copy-done.9 = bf16[2048,512]{1,0:T(8,128)(2,1)S(1)} copy-done((bf16[2048,512]{1,0:T(8,128)(2,1)S(1)}, bf16[2048,512]{1,0:T(8,128)(2,1)}, u32[]{:S(2)}) %copy-start.9) | copy-done | bytes 2097176
  54.5 1.4 %copy-done.15 = bf16[400,2048]{1,0:T(8,128)(2,1)S(1)} copy-done((bf16[400,2048]{1,0:T(8,128)(2,1)S(1)}, bf16[400,2048]{1,0:T(8,128)(2,1)}, u32[]{:S(2)}) %copy-start.15) | copy-done | bytes 1638424
  55.9 4.7 %shard_map.128 = (bf16[384,512]{1,0:T(8,128)(2,1)S(1)}, f32[384,1024]{1,0:T(8,128)S(1)}) custom-call(bf16[400,2048]{1,0:T(8,128)(2,1)S(1)} %copy-done.15, bf16[2048,512]{1,0:T(8,128)(2,1)S(1)} %copy-done.9, bf16[2048,1024]{1,0:T(8,128)(2,1)S(1)} %copy-done.7, bf16[4,1024]{1,0:T(4,128)(2,1)S(1)} %copy-done.12, f32[1,2048]{1,0:T(1,128)S(1)} %bitcast.12), custom_call_target="tpu_custom_call" | custom-call | flops 3000000000 | bytes 1048576 | tf_op jit(solution)/shard_map/pallas_call | solution.py:338
  60.6 1.9 %shard_map.130 = (f32[384,1024]{1,0:T(8,128)S(1)}, f32[384,128]{1,0:T(8,128)S(1)}) custom-call(bf16[384,512]{1,0:T(8,128)(2,1)S(1)} %get-tuple-element.15.query_ref, bf16[384,512]{1,0:T(8,128)(2,1)S(1)} %copy-done.19, bf16[384,1024]{1,0:T(8,128)(2,1)S(1)} %copy-done.17, f32[384,128]{1,0:T(8,128)S(1)} %copy-done.21), custom_call_target="tpu_custom_call" | custom-call | flops 1000000000 | bytes 1048576 | tf_op jit(solution)/shard_map/pallas_call | solution.py:358
  62.5 0.0 copy-start.1
  62.6 0.7 copy-done.1
  63.3 0.7 copy-done.3
  64.0 0.0 all-to-all-done.1
  64.0 2.2 %copy-done = bf16[1024,2048]{1,0:T(8,128)(2,1)S(1)} copy-done((bf16[1024,2048]{1,0:T(8,128)(2,1)S(1)}, bf16[1024,2048]{1,0:T(8,128)(2,1)}, u32[]{:S(2)}) %copy-start) | copy-done | bytes 4194328
  66.2 1.0 %copy-done.2 = bf16[384,512]{1,0:T(8,128)(2,1)S(1)} copy-done((bf16[384,512]{1,0:T(8,128)(2,1)S(1)}, bf16[384,512]{1,0:T(8,128)(2,1)}, u32[]{:S(2)}) %copy-start.2) | copy-done | bytes 393240
  67.2 0.9 %copy-done.4 = f32[384,128]{1,0:T(8,128)S(1)} copy-done((f32[384,128]{1,0:T(8,128)S(1)}, f32[384,128]{1,0:T(8,128)}, u32[]{:S(2)}) %copy-start.4) | copy-done | bytes 196632
  68.1 2.0 %shard_map.132 = bf16[192,2048]{1,0:T(8,128)(2,1)S(1)} custom-call(bf16[384,512]{1,0:T(8,128)(2,1)S(1)} %copy-done.2, f32[384,1024]{1,0:T(8,128)S(1)} %get-tuple-element.16.ogate_ref, bf16[512,384]{1,0:T(8,128)(2,1)S(1)} %bitcast.8, f32[384,1024]{1,0:T(8,128)S(1)} %get-tuple-element.21.numer_ref, f32[384,128]{1,0:T(8,128)S(1)} %copy-done.4, ...), custom_call_target="tpu_custom_call" | custom-call | flops 1000000000 | bytes 1048576 | tf_op jit(solution)/shard_map/pallas_call | solution.py:365
  70.1 2.0 %collective-permute-start.3 = (bf16[192,2048]{1,0:T(8,128)(2,1)S(1)}, bf16[192,2048]{1,0:T(8,128)(2,1)S(1)}, u32[]{:S(2)}, u32[]{:S(2)}) collective-permute-start(bf16[192,2048]{1,0:T(8,128)(2,1)S(1)} %shard_map.132), channel_id=1, source_target_pairs={{0,1},{1,0},{2,3},{3,2},{4,5},{5,4},{6,7},{7,6},{8,9},{9,8},{10,11... | collective-permute-start | bytes 2359304 | tf_op jit(solution)/shard_map/ppermute | solution.py:368
  72.1 2.0 %shard_map.131 = f32[192,2048]{1,0:T(8,128)S(1)} custom-call(bf16[384,512]{1,0:T(8,128)(2,1)S(1)} %copy-done.2, f32[384,1024]{1,0:T(8,128)S(1)} %get-tuple-element.16.ogate_ref, bf16[512,384]{1,0:T(8,128)(2,1)S(1)} %bitcast.9, f32[384,1024]{1,0:T(8,128)S(1)} %get-tuple-element.21.numer_ref, f32[384,128]{1,0:T(8,128)S(1)} %copy-done.4, ...), custom_call_target="tpu_custom_call" | custom-call | flops 1000000000 | bytes 1048576 | tf_op jit(solution)/shard_map/pallas_call | solution.py:369
  74.2 0.0 collective-permute-done.3
  74.2 1.1 %add_convert_fusion = bf16[192,2048]{1,0:T(8,128)(2,1)} fusion(f32[192,2048]{1,0:T(8,128)S(1)} %shard_map.131, bf16[192,2048]{1,0:T(8,128)(2,1)S(1)} %collective-permute-done.3), kind=kLoop, calls=%fused_computation | loop fusion | flops 1179648 | bytes 3145728 | tf_op jit(solution)/shard_map/convert_element_type | solution.py:372
  (24 shorter events, 0.1 us)
Async XLA Ops:
  0.0 8.7 %copy-start.5 = (bf16[192,2048]{1,0:T(8,128)(2,1)S(1)}, bf16[192,2048]{1,0:T(8,128)(2,1)}, u32[]{:S(2)}) copy-start(bf16[192,2048]{1,0:T(8,128)(2,1)} %own_ref.1) | copy-start | bytes 2359300
  0.0 7.5 %copy-start.22 = (f32[2,3,4]{2,0,1:T(2,128)S(1)}, f32[2,3,4]{2,0,1:T(2,128)}, u32[]{:S(2)}) copy-start(f32[2,3,4]{2,0,1:T(2,128)} %param.23) | copy-start | bytes 292
  0.0 8.7 %copy-start.11 = (bf16[4,1024]{1,0:T(4,128)(2,1)S(1)}, bf16[4,1024]{1,0:T(4,128)(2,1)}, u32[]{:S(2)}) copy-start(bf16[4,1024]{1,0:T(4,128)(2,1)} %taps_ref.2) | copy-start | bytes 24580
  0.0 8.7 %copy-start.10 = (f32[2048]{0:T(1024)S(1)}, f32[2048]{0:T(1024)}, u32[]{:S(2)}) copy-start(f32[2048]{0:T(1024)} %param.14) | copy-start | bytes 24580
  0.9 6.7 %collective-permute-start.2 = (bf16[16,2048]{1,0:T(8,128)(2,1)S(1)}, bf16[16,2048]{1,0:T(8,128)(2,1)S(1)}, u32[]{:S(2)}, u32[]{:S(2)}) collective-permute-start(bf16[16,2048]{1,0:T(8,128)(2,1)S(1)} %slice.9), channel_id=1, source_target_pairs={{1,3},{3,5},{5,7},{7,9},{9,11},{11,13},{13,15},{15,17},{17,19},{19... | collective-permute-start | bytes 196616 | tf_op jit(solution)/shard_map/ppermute | solution.py:307
  4.9 2.7 %collective-permute-start.1 = (bf16[16,2048]{1,0:T(8,128)(2,1)S(1)}, bf16[16,2048]{1,0:T(8,128)(2,1)S(1)}, u32[]{:S(2)}, u32[]{:S(2)}) collective-permute-start(bf16[16,2048]{1,0:T(8,128)(2,1)S(1)} %slice.9), channel_id=1, source_target_pairs={{1,2},{3,4},{5,6},{7,8},{9,10},{11,12},{13,14},{15,16},{17,18},{19... | collective-permute-start | bytes 196616 | tf_op jit(solution)/shard_map/ppermute | solution.py:308
  6.2 2.6 %collective-permute-start = (bf16[192,2048]{1,0:T(8,128)(2,1)}, bf16[192,2048]{1,0:T(8,128)(2,1)S(1)}, u32[]{:S(2)}, u32[]{:S(2)}) collective-permute-start(bf16[192,2048]{1,0:T(8,128)(2,1)} %own_ref.1), channel_id=1, source_target_pairs={{0,1},{1,0},{2,3},{3,2},{4,5},{5,4},{6,7},{7,6},{8,9},{9,8},{10,11... | collective-permute-start | bytes 2359304 | tf_op jit(solution)/shard_map/ppermute | solution.py:305
  8.8 2.2 %copy-start.6 = (bf16[2048,1024]{1,0:T(8,128)(2,1)S(1)}, bf16[2048,1024]{1,0:T(8,128)(2,1)}, u32[]{:S(2)}) copy-start(bf16[2048,1024]{1,0:T(8,128)(2,1)} %wv_hbm.1) | copy-start | bytes 12582916
  10.9 1.6 %copy-start.8 = (bf16[2048,512]{1,0:T(8,128)(2,1)S(1)}, bf16[2048,512]{1,0:T(8,128)(2,1)}, u32[]{:S(2)}) copy-start(bf16[2048,512]{1,0:T(8,128)(2,1)} %wk_hbm.1) | copy-start | bytes 6291460
  19.0 1.2 %copy-start.14 = (bf16[400,2048]{1,0:T(8,128)(2,1)}, bf16[400,2048]{1,0:T(8,128)(2,1)S(1)}, u32[]{:S(2)}) copy-start(bf16[400,2048]{1,0:T(8,128)(2,1)S(1)} %get-tuple-element.14.rows_ref) | copy-start | bytes 4915204
  20.2 0.7 copy-start.18
  21.0 0.7 copy-start.20
  21.7 21.9 %copy-start.16 = (bf16[384,1024]{1,0:T(8,128)(2,1)}, bf16[384,1024]{1,0:T(8,128)(2,1)S(1)}, u32[]{:S(2)}) copy-start(bf16[384,1024]{1,0:T(8,128)(2,1)S(1)} %get-tuple-element.19.value_ref) | copy-start | bytes 2359300
  21.7 29.0 %copy-start.12 = (bf16[4,1024]{1,0:T(4,128)(2,1)S(1)}, bf16[4,1024]{1,0:T(4,128)(2,1)}, u32[]{:S(2)}) copy-start(bf16[4,1024]{1,0:T(4,128)(2,1)} %taps_ref.3) | copy-start | bytes 24580
  21.7 29.0 %copy-start.13 = (f32[2048]{0:T(1024)S(1)}, f32[2048]{0:T(1024)}, u32[]{:S(2)}) copy-start(f32[2048]{0:T(1024)} %param.24) | copy-start | bytes 24580
  45.8 18.1 %all-to-all-start.1 = ((bf16[64,8,384]{2,1,0:T(8,128)(2,1)}), bf16[64,8,384]{2,1,0:T(8,128)(2,1)S(1)}, u32[]{:S(2)}, u32[]{:S(2)}) async-start(bf16[64,8,384]{2,1,0:T(8,128)(2,1)} %shard_map.129), calls=%async_computation.1 | async-start | bytes 786432 | tf_op jit(solution)/shard_map/all_to_all | solution.py:357
  50.7 2.2 %copy-start.7 = (bf16[2048,1024]{1,0:T(8,128)(2,1)S(1)}, bf16[2048,1024]{1,0:T(8,128)(2,1)}, u32[]{:S(2)}) copy-start(bf16[2048,1024]{1,0:T(8,128)(2,1)} %wo_hbm.1) | copy-start | bytes 12582916
  52.9 1.6 %copy-start.9 = (bf16[2048,512]{1,0:T(8,128)(2,1)S(1)}, bf16[2048,512]{1,0:T(8,128)(2,1)}, u32[]{:S(2)}) copy-start(bf16[2048,512]{1,0:T(8,128)(2,1)} %wq_hbm.1) | copy-start | bytes 6291460
  54.5 1.4 %copy-start.15 = (bf16[400,2048]{1,0:T(8,128)(2,1)S(1)}, bf16[400,2048]{1,0:T(8,128)(2,1)}, u32[]{:S(2)}) copy-start(bf16[400,2048]{1,0:T(8,128)(2,1)} %copy-done.14) | copy-start | bytes 4915204
  55.9 4.7 %copy-start.17 = (bf16[384,1024]{1,0:T(8,128)(2,1)S(1)}, bf16[384,1024]{1,0:T(8,128)(2,1)}, u32[]{:S(2)}) copy-start(bf16[384,1024]{1,0:T(8,128)(2,1)} %copy-done.16) | copy-start | bytes 2359300
  55.9 4.7 %copy-start.19 = (bf16[384,512]{1,0:T(8,128)(2,1)S(1)}, bf16[384,512]{1,0:T(8,128)(2,1)}, u32[]{:S(2)}) copy-start(bf16[384,512]{1,0:T(8,128)(2,1)} %copy-done.18) | copy-start | bytes 1179652
  55.9 4.7 %copy-start.21 = (f32[384,128]{1,0:T(8,128)S(1)}, f32[384,128]{1,0:T(8,128)}, u32[]{:S(2)}) copy-start(f32[384,128]{1,0:T(8,128)} %copy-done.20) | copy-start | bytes 589828
  62.5 0.7 copy-start.1
  63.3 0.7 copy-start.3
  64.0 2.2 %copy-start = (bf16[1024,2048]{1,0:T(8,128)(2,1)S(1)}, bf16[1024,2048]{1,0:T(8,128)(2,1)}, u32[]{:S(2)}) copy-start(bf16[1024,2048]{1,0:T(8,128)(2,1)} %wout_ref.3) | copy-start | bytes 12582916
  66.2 1.0 %copy-start.2 = (bf16[384,512]{1,0:T(8,128)(2,1)S(1)}, bf16[384,512]{1,0:T(8,128)(2,1)}, u32[]{:S(2)}) copy-start(bf16[384,512]{1,0:T(8,128)(2,1)} %copy-done.1) | copy-start | bytes 1179652
  67.2 0.9 %copy-start.4 = (f32[384,128]{1,0:T(8,128)S(1)}, f32[384,128]{1,0:T(8,128)}, u32[]{:S(2)}) copy-start(f32[384,128]{1,0:T(8,128)} %copy-done.3) | copy-start | bytes 589828
  70.1 4.1 %collective-permute-start.3 = (bf16[192,2048]{1,0:T(8,128)(2,1)S(1)}, bf16[192,2048]{1,0:T(8,128)(2,1)S(1)}, u32[]{:S(2)}, u32[]{:S(2)}) collective-permute-start(bf16[192,2048]{1,0:T(8,128)(2,1)S(1)} %shard_map.132), channel_id=1, source_target_pairs={{0,1},{1,0},{2,3},{3,2},{4,5},{5,4},{6,7},{7,6},{8,9},{9,8},{10,11... | collective-permute-start | bytes 2359304 | tf_op jit(solution)/shard_map/ppermute | solution.py:368

commit v2 on v1

--- a/solution.py
+++ b/solution.py
@@ -27,24 +27,35 @@
 MIB = 1 << 20
 
 
-def in_vmem():
-    return pl.BlockSpec(memory_space=pltpu.VMEM)
-
-
-def in_hbm():
-    return pl.BlockSpec(memory_space=pl.ANY)
-
-
-def call(kernel, outs, ins, scratch=(), flops=0, limit=40):
-    return pl.pallas_call(
+def call(kernel, outs, out_spaces, spaces, scratch=(), flops=0, limit=8):
+    def spec(space):
+        return pl.BlockSpec(memory_space=pltpu.VMEM if space is None else space)
+
+    def placed(like, space):
+        return like if space is None else space(like.shape, like.dtype)
+
+    several = isinstance(outs, tuple)
+    run = pl.pallas_call(
         kernel,
-        out_shape=outs,
-        in_specs=ins,
-        out_specs=jax.tree.map(lambda _: in_vmem(), outs),
+        out_shape=tuple(map(placed, outs, out_spaces)) if several else placed(outs, out_spaces),
+        in_specs=[spec(space) for space in spaces],
+        out_specs=tuple(map(spec, out_spaces)) if several else spec(out_spaces),
         scratch_shapes=list(scratch),
         cost_estimate=pl.CostEstimate(flops=flops, transcendentals=0, bytes_accessed=1 << 20),
         compiler_params=pltpu.CompilerParams(vmem_limit_bytes=limit * MIB),
     )
+
+    def kept(x, space):
+        return x if space is None else pltpu.with_memory_space_constraint(x, space)
+
+    return lambda *args: run(*map(kept, args, spaces))
+
+
+def started(pairs, sems):
+    copies = [pltpu.make_async_copy(src, dst, sems.at[n]) for n, (src, dst) in enumerate(pairs)]
+    for copy in copies:
+        copy.start()
+    return copies
 
 
 def thirds(x):
@@ -67,14 +78,20 @@
 
 
 def summary_kernel(own_ref, oth_ref, one_ref, two_ref, gain_ref, wk_hbm, wv_hbm, wg_ref, taps_ref, offs_ref,
-                   key_ref, value_ref, logs_ref, piece_ref, rows_ref, wk_ref, wv_ref, pre_ref, sems):
+                   key_out, value_out, logs_out, piece_ref, rows_out,
+                   key_ref, value_ref, logs_ref, rows_ref, wk_ref, wv_ref, pre_ref, sems, out_sems):
     wide = HEADS * DV // 2
-    copies = [pltpu.make_async_copy(wk_hbm, wk_ref, sems.at[0])]
-    for c in range(2):
-        cols = pl.ds(c * wide, wide)
-        copies.append(pltpu.make_async_copy(wv_hbm.at[:, cols], wv_ref.at[:, cols], sems.at[1 + c]))
-    for copy in copies:
-        copy.start()
+    copies = started(
+        [(wk_hbm, wk_ref)]
+        + [(wv_hbm.at[:, pl.ds(c * wide, wide)], wv_ref.at[:, pl.ds(c * wide, wide)]) for c in range(2)],
+        sems,
+    )
+    outs = [
+        pltpu.make_async_copy(src, dst, out_sems.at[n])
+        for n, (src, dst) in enumerate(
+            [(rows_ref, rows_out), (logs_ref, logs_out), (key_ref, key_out), (value_ref, value_out)]
+        )
+    ]
     tp = lax.axis_index("tp")
     gain = gain_ref[...]
 
@@ -88,6 +105,7 @@
         for part in range(HALF // 48):
             to = pl.multiple_of(TAIL + at * HALF + part * 48, 16)
             rows_ref[pl.ds(to, 48), :] = normalized(ref[part * 48 : part * 48 + 48, :])
+    outs[0].start()
     own = pl.ds(TAIL, ROWS)
     gates = jnp.dot(rows_ref[own, :], wg_ref[...], preferred_element_type=F32)
     copies[0].wait()
@@ -105,6 +123,7 @@
         gate.append(g)
         inside.append(total)
         totals.append(total[SPAN - 1 : SPAN, :])
+    outs[1].start()
     write, level = [], None
     later = jnp.zeros_like(totals[0])
     for b in reversed(range(BLOCKS)):
@@ -122,10 +141,12 @@
         for b in range(BLOCKS):
             rows = slice(b * SPAN, (b + 1) * SPAN)
             key_ref[rows, lanes] = (mixed_rows(pre_ref, taps, lanes, b * SPAN, SPAN) * DQK**-0.5).astype(BF)
+    outs[2].start()
     for c in range(2):
         copies[1 + c].wait()
         cols = slice(c * wide, (c + 1) * wide)
         value_ref[:, cols] = jnp.dot(rows_ref[own, :], wv_ref[:, cols], preferred_element_type=F32).astype(BF)
+    outs[3].start()
     ones = jnp.ones((ROWS, 128), BF)
     dims = (((0,), (0,)), ((), ()))
     for h in range(HEADS):
@@ -144,6 +165,8 @@
         out = slice(h * DQK, (h + 1) * DQK)
         piece_ref[out, :DV] = memory.astype(BF)
         piece_ref[out, DV:] = extra.astype(BF)
+    for copy in outs:
+        copy.wait()
 
 
 def prefix_kernel(piece_ref, out_ref, wide_ref, done_ref):
@@ -177,32 +200,26 @@
     out_ref[...] = done_ref[...].astype(BF)
 
 
-def query_kernel(rows_ref, wq_hbm, wo_hbm, taps_ref, gain_ref, query_ref, ogate_ref, wq_ref, wo_ref, pre_ref, sems):
-    wide = HEADS * DV // 2
-    copies = [pltpu.make_async_copy(wq_hbm, wq_ref, sems.at[0])]
-    for c in range(2):
-        cols = pl.ds(c * wide, wide)
-        copies.append(pltpu.make_async_copy(wo_hbm.at[:, cols], wo_ref.at[:, cols], sems.at[1 + c]))
-    for copy in copies:
-        copy.start()
+def local_kernel(rows_hbm, wq_hbm, key_hbm, value_hbm, logs_hbm, taps_ref,
+                 query_out, numer_out, stats_out,
+                 rows_ref, wq_ref, key_ref, value_ref, logs_ref, pre_ref, query_ref, numer_ref, stats_ref, sems, out_sems):
+    copies = started(
+        [(rows_hbm, rows_ref), (wq_hbm, wq_ref), (logs_hbm, logs_ref), (key_hbm, key_ref), (value_hbm, value_ref)], sems
+    )
     tp = lax.axis_index("tp")
     taps = taps_ref[:, pl.ds(pl.multiple_of(tp * (HEADS * DQK), 128), HEADS * DQK)].astype(F32)
-    gain = gain_ref[:, pl.ds(pl.multiple_of(tp * (HEADS * DV), 128), HEADS * DV)]
     copies[0].wait()
+    copies[1].wait()
     pre_ref[...] = jnp.dot(rows_ref[...], wq_ref[...], preferred_element_type=F32).astype(BF).astype(F32)
     for h in range(HEADS):
         lanes = slice(h * DQK, (h + 1) * DQK)
         for b in range(BLOCKS):
             rows = slice(b * SPAN, (b + 1) * SPAN)
             query_ref[rows, lanes] = mixed_rows(pre_ref, taps, lanes, b * SPAN, SPAN).astype(BF)
-    for c in range(2):
-        copies[1 + c].wait()
-        cols = slice(c * wide, (c + 1) * wide)
-        pre = jnp.dot(rows_ref[pl.ds(TAIL, ROWS), :], wo_ref[:, cols], preferred_element_type=F32).astype(BF).astype(F32)
-        ogate_ref[:, cols] = gain[:, cols] / (1.0 + jnp.exp(-pre))
-
-
-def local_kernel(query_ref, key_ref, value_ref, logs_ref, numer_ref, stats_ref):
+    outs = [pltpu.make_async_copy(query_ref, query_out, out_sems.at[0])]
+    outs[0].start()
+    for copy in copies[2:]:
+        copy.wait()
     lane = lane_of((SPAN, 128))
     cols = [logs_ref[b * SPAN : (b + 1) * SPAN, :] for b in range(BLOCKS)]
     flat = [c.T for c in cols]
@@ -217,6 +234,7 @@
     nt = (((1,), (1,)), ((), ()))
     for h in range(HEADS):
         head = slice(h * DQK, (h + 1) * DQK)
+        wide = slice(h * DV, (h + 1) * DV)
         for t in range(BLOCKS):
             rows = slice(t * SPAN, (t + 1) * SPAN)
             seen = (t + 1) * SPAN
@@ -241,12 +259,41 @@
                 lax.dot_general(query_ref[rows, head], key_ref[:seen, head], nt, preferred_element_type=F32) * weight
             )
             denom = jnp.sum(scores, axis=1, keepdims=True)
-            numer_ref[rows, h * DV : (h + 1) * DV] = jnp.dot(
-                scores.astype(BF), value_ref[:seen, h * DV : (h + 1) * DV], preferred_element_type=F32
+            numer_ref[rows, wide] = jnp.dot(scores.astype(BF), value_ref[:seen, wide], preferred_element_type=F32)
+            stats[t] = jnp.where(lane == h, denom, jnp.where(lane == HEADS + h, top, stats[t]))
+        outs.append(
+            pltpu.make_async_copy(
+                numer_ref.at[:, pl.ds(h * DV, DV)], numer_out.at[:, pl.ds(h * DV, DV)], out_sems.at[1 + h]
             )
-            stats[t] = jnp.where(lane == h, denom, jnp.where(lane == HEADS + h, top, stats[t]))
+        )
+        outs[-1].start()
     for t in range(BLOCKS):
         stats_ref[t * SPAN : (t + 1) * SPAN, :] = stats[t]
+    outs.append(pltpu.make_async_copy(stats_ref, stats_out, out_sems.at[1 + HEADS]))
+    outs[-1].start()
+    for copy in outs:
+        copy.wait()
+
+
+def gate_kernel(rows_hbm, wo_hbm, gain_ref, query_hbm, numer_hbm, stats_hbm, wout_hbm,
+                ogate_ref, query_ref, numer_ref, stats_ref, wout_ref, rows_ref, wo_ref, sems):
+    wide = HEADS * DV // 2
+    copies = started(
+        [(rows_hbm, rows_ref)]
+        + [(wo_hbm.at[:, pl.ds(c * wide, wide)], wo_ref.at[:, pl.ds(c * wide, wide)]) for c in range(2)]
+        + [(query_hbm, query_ref), (numer_hbm, numer_ref), (stats_hbm, stats_ref), (wout_hbm, wout_ref)],
+        sems,
+    )
+    tp = lax.axis_index("tp")
+    gain = gain_ref[:, pl.ds(pl.multiple_of(tp * (HEADS * DV), 128), HEADS * DV)]
+    copies[0].wait()
+    for c in range(2):
+        copies[1 + c].wait()
+        cols = slice(c * wide, (c + 1) * wide)
+        pre = jnp.dot(rows_ref[pl.ds(TAIL, ROWS), :], wo_ref[:, cols], preferred_element_type=F32).astype(BF).astype(F32)
+        ogate_ref[:, cols] = gain[:, cols] / (1.0 + jnp.exp(-pre))
+    for copy in copies[3:]:
+        copy.wait()
 
 
 def hidden_rows(first, query_ref, ogate_ref, state_ref, numer_ref, stats_ref, hidden_ref):
@@ -314,60 +361,61 @@
     offsets = jnp.pad(offsets, ((0, 0), (0, 128 - 2 * HEADS)))
     gain = norm_gain.reshape(1, -1)
     head_gain = head_gain.reshape(1, -1)
-    v, m = in_vmem(), in_hbm()
+    v, m, n = pltpu.VMEM, pltpu.HBM, None
+    dma = pltpu.SemaphoreType.DMA
+    key_shape, value_shape = shape((ROWS, HEADS * DQK), BF), shape((ROWS, HEADS * DV), BF)
+    logs_shape, wide_shape = shape((ROWS, 128), F32), shape((ROWS, HEADS * DV), F32)
+    rows_shape, pre_shape = shape((TAIL + ROWS, width), BF), shape((TAIL + ROWS, HEADS * DQK), F32)
+
+    def room(like):
+        return pltpu.VMEM(like.shape, like.dtype)
+
     key, value, logs, pieces, rows = call(
         summary_kernel,
-        (
-            shape((ROWS, HEADS * DQK), BF),
-            shape((ROWS, HEADS * DV), BF),
-            shape((ROWS, 128), F32),
-            shape((HEADS * DQK, WIDTH), BF),
-            shape((TAIL + ROWS, width), BF),
-        ),
-        [v, v, v, v, v, m, m, v, v, v],
-        [
-            pltpu.VMEM((width, HEADS * DQK), BF),
-            pltpu.VMEM((width, HEADS * DV), BF),
-            pltpu.VMEM((TAIL + ROWS, HEADS * DQK), F32),
-            pltpu.SemaphoreType.DMA((3,)),
-        ],
+        (key_shape, value_shape, logs_shape, shape((HEADS * DQK, WIDTH), BF), rows_shape),
+        (m, m, m, n, m),
+        [n, n, n, n, n, m, m, n, n, n],
+        [room(key_shape), room(value_shape), room(logs_shape), room(rows_shape), room(w_key), room(w_value), room(pre_shape), dma((3,)), dma((4,))],
         flops=3_000_000_000,
+        limit=20,
     )(tokens, other, to_first, to_second, gain, w_key, w_value, w_gates, conv_key, offsets)
-    pieces = pieces.reshape(stretches, 8, WIDTH)
-    pieces = lax.all_to_all(pieces, SP, 0, 0, tiled=True)
-    query, ogate = call(
-        query_kernel,
-        (shape((ROWS, HEADS * DQK), BF), shape((ROWS, HEADS * DV), F32)),
-        [v, m, m, v, v],
-        [
-            pltpu.VMEM((width, HEADS * DQK), BF),
-            pltpu.VMEM((width, HEADS * DV), BF),
-            pltpu.VMEM((TAIL + ROWS, HEADS * DQK), F32),
-            pltpu.SemaphoreType.DMA((3,)),
-        ],
+    pieces = lax.all_to_all(pieces.reshape(stretches, 8, WIDTH), SP, 0, 0, tiled=True)
+    query, numer, stats = call(
+        local_kernel,
+        (key_shape, wide_shape, logs_shape),
+        (m, m, m),
+        [m, m, m, m, m, n],
+        [room(rows_shape), room(w_query), room(key_shape), room(value_shape), room(logs_shape), room(pre_shape), room(key_shape), room(wide_shape), room(logs_shape), dma((5,)), dma((2 + HEADS,))],
         flops=3_000_000_000,
-    )(rows, w_query, w_ogate, conv_query, head_gain)
+        limit=16,
+    )(rows, w_query, key, value, logs, conv_query)
+    pieces, query, numer, stats = lax.optimization_barrier((pieces, query, numer, stats))
     state = call(
         prefix_kernel,
         shape((stretches, 8, WIDTH), BF),
-        [v],
+        n,
+        [n],
         [pltpu.VMEM((stretches, 8, WIDTH), F32), pltpu.VMEM((stretches, 8, WIDTH), F32)],
         flops=100_000_000,
     )(pieces)
+    state, query, numer, stats = lax.optimization_barrier((state, query, numer, stats))
     state = lax.all_to_all(state, SP, 0, 0, tiled=True).reshape(HEADS * DQK, WIDTH)
-    numer, stats = call(
-        local_kernel,
-        (shape((ROWS, HEADS * DV), F32), shape((ROWS, 128), F32)),
-        [v, v, v, v],
-        flops=1_000_000_000,
-    )(query, key, value, logs)
+    ogate, query, numer, stats, w_last = call(
+        gate_kernel,
+        (wide_shape, key_shape, wide_shape, logs_shape, shape(w_out.shape, BF)),
+        (v, v, v, v, v),
+        [m, m, n, m, m, m, m],
+        [room(rows_shape), room(w_ogate), dma((7,))],
+        flops=3_000_000_000,
+        limit=10,
+    )(rows, w_ogate, head_gain, query, numer, stats, w_out)
     hidden = pltpu.VMEM((HALF, HEADS * DV), BF)
-    sent = call(sent_kernel, shape((HALF, width), BF), [v] * 6, [hidden], flops=1_000_000_000)(
-        query, ogate, state, numer, stats, w_out
+    sent = call(sent_kernel, shape((HALF, width), BF), n, [v, v, n, v, v, v], [hidden], flops=1_000_000_000, limit=8)(
+        query, ogate, state, numer, stats, w_last
     )
     got = lax.ppermute(sent, "tp", [(0, 1), (1, 0)])
-    kept = call(kept_kernel, shape((HALF, width), F32), [v] * 6, [hidden], flops=1_000_000_000)(
-        query, ogate, state, numer, stats, w_out
+    kept = call(kept_kernel, shape((HALF, width), F32), n, [v, v, n, v, v, v], [hidden], flops=1_000_000_000, limit=8)(
+        query, ogate, state, numer, stats, w_last
     )
     return (kept + got.astype(F32)).astype(BF)
 

time: 75.9 us -> 70.3 us (0.926)
  blocking collectives: 21.9 us -> 0 us
  starting transfers between devices: 12.1 us -> 23.9 us
  local copies, waits for them, and re-layouts: 19.3 us -> 9.6 us
  Pallas kernels: 19.4 us -> 26.7 us
  waiting for transfers between devices: 1.15 us -> 8.2 us
    all_to_all x1 -> x0, blocking collectives: 21.9 us -> none  [body(): pieces = lax.all_to_all(pieces, SP, 0, 0, tiled=True)]
    all_to_all x0 -> x1, starting transfers between devices: none -> 10.9 us  [body(): lax.all_to_all(pieces.reshape(stretches, 8, WIDTH), SP, 0, 0, tiled=True)]
    unnamed x47 -> x25, local copies, waits for them, and re-layouts: 17.2 us -> 7.51 us
    pallas_call x6, Pallas kernels: 19.4 us -> 26.7 us  [call(): return lambda *args: run(*map(kept, args, spaces))]
    all_to_all x0 -> x1, waiting for transfers between devices: none -> 4.4 us  [body(): lax.all_to_all(pieces.reshape(stretches, 8, WIDTH), SP, 0, 0, tiled=True)]
    all_to_all x1, waiting for transfers between devices: 0.01 us -> 2.65 us  [body(): lax.all_to_all(state, SP, 0, 0, tiled=True).reshape(HEADS * DQK, WIDTH)]
    all_to_all x1, starting transfers between devices: 4.81 us -> 5.57 us  [body(): lax.all_to_all(state, SP, 0, 0, tiled=True).reshape(HEADS * DQK, WIDTH)]
  transfers between devices with their start and end apart: 5 -> 6, of which waited for: 1 -> 3; matrix products, arithmetic and copies ran while one was open for 2% -> 2% of each run, Pallas kernels for 11% -> 19%
where the time goes in v2:
time: 70.3 us; the launch traced here: 69.8 us
  Pallas kernels  26.7 us (38%)
  starting transfers between devices  23.9 us (34%)
  local copies, waits for them, and re-layouts  9.6 us (14%)
  waiting for transfers between devices  8.2 us (12%)
  other arithmetic  1.19 us (2%)
    pallas_call x6, Pallas kernels, call(): return lambda *args: run(*map(kept, args, spaces))  26.7 us
    all_to_all x1, starting transfers between devices, body(): lax.all_to_all(pieces.reshape(stretches, 8, WIDTH), SP, 0, 0, tiled=True)  10.9 us
    unnamed x25, local copies, waits for them, and re-layouts  7.51 us
    all_to_all x1, starting transfers between devices, body(): lax.all_to_all(state, SP, 0, 0, tiled=True).reshape(HEADS * DQK, WIDTH)  5.57 us
    all_to_all x1, waiting for transfers between devices, body(): lax.all_to_all(pieces.reshape(stretches, 8, WIDTH), SP, 0, 0, tiled=True)  4.4 us
    ppermute x1, starting transfers between devices, body(): lax.ppermute(last, SP_TP, [(2 * i + 1, 2 * i + 3) for i in range(stretche...  3.92 us
    all_to_all x1, waiting for transfers between devices, body(): lax.all_to_all(state, SP, 0, 0, tiled=True).reshape(HEADS * DQK, WIDTH)  2.65 us
    ppermute x1, starting transfers between devices, body(): got = lax.ppermute(sent, 'tp', [(0, 1), (1, 0)])  2.17 us
  transfers between devices with their start and end apart: 6, of which 3 were waited for; matrix products, arithmetic and copies ran while one was open for 2% of the time, Pallas kernels for 19%

profile of v2, /device:TPU:1, one launch (start us, length us, event | category | flops | bytes accessed | tf_op | source)
XLA Modules:
  0.0 69.8 jit_solution(9080338012449206000)
XLA Ops:
  0.0 0.0 copy-start.7
  0.0 0.0 copy-start.11
  0.0 0.0 copy-start.9
  0.0 0.0 copy-start.8
  0.0 0.9 %slice.9 = bf16[16,2048]{1,0:T(8,128)(2,1)S(1)} slice(bf16[192,2048]{1,0:T(8,128)(2,1)} %own_ref.1), slice={[176:192], [0:2048]} | slice | bytes 131072 | tf_op jit(solution)/shard_map/slice | solution.py:353
  0.9 3.9 %collective-permute-start.2 = (bf16[16,2048]{1,0:T(8,128)(2,1)S(1)}, bf16[16,2048]{1,0:T(8,128)(2,1)S(1)}, u32[]{:S(2)}, u32[]{:S(2)}) collective-permute-start(bf16[16,2048]{1,0:T(8,128)(2,1)S(1)} %slice.9), channel_id=1, source_target_pairs={{1,3},{3,5},{5,7},{7,9},{9,11},{11,13},{13,15},{15,17},{17,19},{19... | collective-permute-start | bytes 196616 | tf_op jit(solution)/shard_map/ppermute | solution.py:354
  4.9 1.3 %collective-permute-start.1 = (bf16[16,2048]{1,0:T(8,128)(2,1)S(1)}, bf16[16,2048]{1,0:T(8,128)(2,1)S(1)}, u32[]{:S(2)}, u32[]{:S(2)}) collective-permute-start(bf16[16,2048]{1,0:T(8,128)(2,1)S(1)} %slice.9), channel_id=1, source_target_pairs={{1,2},{3,4},{5,6},{7,8},{9,10},{11,12},{13,14},{15,16},{17,18},{19... | collective-permute-start | bytes 196616 | tf_op jit(solution)/shard_map/ppermute | solution.py:355
  6.2 0.1 collective-permute-start
  6.3 0.8 %constant_dynamic-slice_fusion = (bf16[2048,4]{0,1:T(4,128)(2,1)S(1)}, bf16[2048,4]{0,1:T(4,128)(2,1)S(1)}) fusion(bf16[2048,8]{0,1:T(8,128)(2,1)} %param.20, s32[]{:T(128)S(6)} %select_n.4, bf16[2048,8]{0,1:T(8,128)(2,1)} %param.19), kind=kLoop, calls=%fused_computation.6 | loop fusion | bytes 65540 | tf_op jit(solution)/shard_map/dynamic_slice | solution.py:357
  7.1 0.3 copy.18
  7.4 0.1 pad.8.wg_ref
  7.5 0.0 copy-done.11
  7.5 0.1 select_maximum_fusion.offs_ref
  7.6 0.0 collective-permute-done.2.two_ref
  7.6 0.0 collective-permute-done.1.one_ref
  7.6 1.1 %collective-permute-done.oth_ref = bf16[192,2048]{1,0:T(8,128)(2,1)S(1)} collective-permute-done((bf16[192,2048]{1,0:T(8,128)(2,1)}, bf16[192,2048]{1,0:T(8,128)(2,1)S(1)}, u32[]{:S(2)}, u32[]{:S(2)}) %collective-permute-start) | collective-permute-done | bytes 786464 | tf_op jit(solution)/shard_map/ppermute | solution.py:352
  8.7 0.0 copy-done.7
  8.7 0.0 copy-done.9
  8.8 0.0 copy-done.8
  8.8 0.0 copy-start.10
  8.8 9.1 %shard_map.127 = (bf16[384,512]{1,0:T(8,128)(2,1)}, bf16[384,1024]{1,0:T(8,128)(2,1)}, f32[384,128]{1,0:T(8,128)}, bf16[512,384]{1,0:T(8,128)(2,1)}, bf16[400,2048]{1,0:T(8,128)(2,1)}) custom-call(bf16[192,2048]{1,0:T(8,128)(2,1)S(1)} %copy-done.7, bf16[192,2048]{1,0:T(8,128)(2,1)S(1)} %collective-permute-done.oth_ref, ...), custom_call_target="tpu_custom_call" | custom-call | flops 3000000000 | bytes 1048576 | tf_op jit(solution)/shard_map/pallas_call | solution.py:51
  17.8 10.9 %all-to-all-start = ((bf16[64,8,384]{2,1,0:T(8,128)(2,1)}), bf16[64,8,384]{2,1,0:T(8,128)(2,1)S(1)}, u32[]{:S(2)}, u32[]{:S(2)}) async-start(bf16[64,8,384]{2,1,0:T(8,128)(2,1)} %bitcast.2), calls=%async_computation | async-start | bytes 786432 | tf_op jit(solution)/shard_map/all_to_all | solution.py:382
  28.7 0.0 copy-done.10
  28.7 0.0 copy-start.6
  28.7 6.7 %shard_map.128 = (bf16[384,512]{1,0:T(8,128)(2,1)}, f32[384,1024]{1,0:T(8,128)}, f32[384,128]{1,0:T(8,128)}) custom-call(bf16[400,2048]{1,0:T(8,128)(2,1)} %get-tuple-element.26.rows_hbm, bf16[2048,512]{1,0:T(8,128)(2,1)} %wq_hbm.1, bf16[384,512]{1,0:T(8,128)(2,1)} %get-tuple-element.28.key_hbm, bf16[384,1024]{1,0:T(8,128)(2,1)} %get-tuple-element.29.value_hbm, ...), custom_call_target="tpu_custom_call" | custom-call | flops 3000000000 | bytes 1048576 | tf_op jit(solution)/shard_map/pallas_call | solution.py:51
  35.5 4.4 %all-to-all-done.piece_ref = bf16[64,8,384]{2,1,0:T(8,128)(2,1)S(1)} async-done(((bf16[64,8,384]{2,1,0:T(8,128)(2,1)}), bf16[64,8,384]{2,1,0:T(8,128)(2,1)S(1)}, u32[]{:S(2)}, u32[]{:S(2)}) %all-to-all-start) | async-done | bytes 393248 | tf_op jit(solution)/shard_map/all_to_all | solution.py:382
  39.9 2.2 %shard_map.129 = bf16[64,8,384]{2,1,0:T(8,128)(2,1)} custom-call(bf16[64,8,384]{2,1,0:T(8,128)(2,1)S(1)} %all-to-all-done.piece_ref), custom_call_target="tpu_custom_call" | custom-call | flops 100000000 | bytes 1048576 | tf_op jit(solution)/shard_map/pallas_call | solution.py:51
  42.1 5.6 %all-to-all-start.1 = ((bf16[64,8,384]{2,1,0:T(8,128)(2,1)}), bf16[64,8,384]{2,1,0:T(8,128)(2,1)S(1)}, u32[]{:S(2)}, u32[]{:S(2)}) async-start(bf16[64,8,384]{2,1,0:T(8,128)(2,1)} %shard_map.129), calls=%async_computation.1 | async-start | bytes 786432 | tf_op jit(solution)/shard_map/all_to_all | solution.py:402
  47.7 0.0 copy-done.6
  47.7 4.6 %shard_map.130 = (f32[384,1024]{1,0:T(8,128)S(1)}, bf16[384,512]{1,0:T(8,128)(2,1)S(1)}, f32[384,1024]{1,0:T(8,128)S(1)}, f32[384,128]{1,0:T(8,128)S(1)}, bf16[1024,2048]{1,0:T(8,128)(2,1)S(1)}) custom-call(bf16[400,2048]{1,0:T(8,128)(2,1)} %get-tuple-element.26.rows_hbm, bf16[2048,1024]{1,0:T(8,128)(2,1)} %wo_hbm.1, f32[1,2048]{1,0:T(1,128)S(1)} %bitcast.10, ...), custom_call_target="tpu_custom_call" | custom-call | flops 3000000000 | bytes 1048576 | tf_op jit(solution)/shard_map/pallas_call | solution.py:51
  52.3 0.0 copy-start
  52.3 1.9 %copy-done = bf16[1024,2048]{1,0:T(8,128)(2,1)} copy-done((bf16[1024,2048]{1,0:T(8,128)(2,1)}, bf16[1024,2048]{1,0:T(8,128)(2,1)S(1)}, u32[]{:S(2)}) %copy-start) | copy-done | bytes 4194328
  54.3 0.0 copy-start.2
  54.3 0.7 %copy-done.2 = bf16[384,512]{1,0:T(8,128)(2,1)} copy-done((bf16[384,512]{1,0:T(8,128)(2,1)}, bf16[384,512]{1,0:T(8,128)(2,1)S(1)}, u32[]{:S(2)}) %copy-start.2) | copy-done | bytes 393240
  55.0 0.0 copy-start.4
  55.0 0.7 copy-done.4
  55.7 2.6 %all-to-all-done.1 = bf16[64,8,384]{2,1,0:T(8,128)(2,1)S(1)} async-done(((bf16[64,8,384]{2,1,0:T(8,128)(2,1)}), bf16[64,8,384]{2,1,0:T(8,128)(2,1)S(1)}, u32[]{:S(2)}, u32[]{:S(2)}) %all-to-all-start.1) | async-done | bytes 393248 | tf_op jit(solution)/shard_map/all_to_all | solution.py:402
  58.3 0.0 copy-start.1
  58.3 2.2 %copy-done.1 = bf16[1024,2048]{1,0:T(8,128)(2,1)S(1)} copy-done((bf16[1024,2048]{1,0:T(8,128)(2,1)S(1)}, bf16[1024,2048]{1,0:T(8,128)(2,1)}, u32[]{:S(2)}) %copy-start.1) | copy-done | bytes 4194328
  60.5 0.0 copy-start.3
  60.5 1.0 %copy-done.3 = bf16[384,512]{1,0:T(8,128)(2,1)S(1)} copy-done((bf16[384,512]{1,0:T(8,128)(2,1)S(1)}, bf16[384,512]{1,0:T(8,128)(2,1)}, u32[]{:S(2)}) %copy-start.3) | copy-done | bytes 393240
  61.5 0.0 copy-start.5
  61.5 0.9 %copy-done.5 = f32[384,128]{1,0:T(8,128)S(1)} copy-done((f32[384,128]{1,0:T(8,128)S(1)}, f32[384,128]{1,0:T(8,128)}, u32[]{:S(2)}) %copy-start.5) | copy-done | bytes 196632
  62.5 2.0 %shard_map.132 = bf16[192,2048]{1,0:T(8,128)(2,1)S(1)} custom-call(bf16[384,512]{1,0:T(8,128)(2,1)S(1)} %copy-done.3, f32[384,1024]{1,0:T(8,128)S(1)} %get-tuple-element.42.ogate_ref, bf16[512,384]{1,0:T(8,128)(2,1)S(1)} %bitcast.8, f32[384,1024]{1,0:T(8,128)S(1)} %get-tuple-element.44.numer_ref, f32[384,128]{1,0:T(8,128)S(1)} %copy-done.5, ...), custom_call_target="tpu_custom_call" | custom-call | flops 1000000000 | bytes 1048576 | tf_op jit(solution)/shard_map/pallas_call | solution.py:51
  64.5 2.2 %collective-permute-start.3 = (bf16[192,2048]{1,0:T(8,128)(2,1)S(1)}, bf16[192,2048]{1,0:T(8,128)(2,1)S(1)}, u32[]{:S(2)}, u32[]{:S(2)}) collective-permute-start(bf16[192,2048]{1,0:T(8,128)(2,1)S(1)} %shard_map.132), channel_id=1, source_target_pairs={{0,1},{1,0},{2,3},{3,2},{4,5},{5,4},{6,7},{7,6},{8,9},{9,8},{10,11... | collective-permute-start | bytes 2359304 | tf_op jit(solution)/shard_map/ppermute | solution.py:416
  66.7 2.0 %shard_map.131 = f32[192,2048]{1,0:T(8,128)S(1)} custom-call(bf16[384,512]{1,0:T(8,128)(2,1)S(1)} %copy-done.3, f32[384,1024]{1,0:T(8,128)S(1)} %get-tuple-element.42.ogate_ref, bf16[512,384]{1,0:T(8,128)(2,1)S(1)} %bitcast.9, f32[384,1024]{1,0:T(8,128)S(1)} %get-tuple-element.44.numer_ref, f32[384,128]{1,0:T(8,128)S(1)} %copy-done.5, ...), custom_call_target="tpu_custom_call" | custom-call | flops 1000000000 | bytes 1048576 | tf_op jit(solution)/shard_map/pallas_call | solution.py:51
  68.7 0.0 collective-permute-done.3
  68.7 1.1 %add_convert_fusion = bf16[192,2048]{1,0:T(8,128)(2,1)} fusion(f32[192,2048]{1,0:T(8,128)S(1)} %shard_map.131, bf16[192,2048]{1,0:T(8,128)(2,1)S(1)} %collective-permute-done.3), kind=kLoop, calls=%fused_computation | loop fusion | flops 1179648 | bytes 3145728 | tf_op jit(solution)/shard_map/convert_element_type | solution.py:420
  (3 shorter events, 0.0 us)
Async XLA Ops:
  0.0 8.7 %copy-start.7 = (bf16[192,2048]{1,0:T(8,128)(2,1)S(1)}, bf16[192,2048]{1,0:T(8,128)(2,1)}, u32[]{:S(2)}) copy-start(bf16[192,2048]{1,0:T(8,128)(2,1)} %own_ref.1) | copy-start | bytes 2359300
  0.0 7.5 %copy-start.11 = (f32[2,3,4]{2,0,1:T(2,128)S(1)}, f32[2,3,4]{2,0,1:T(2,128)}, u32[]{:S(2)}) copy-start(f32[2,3,4]{2,0,1:T(2,128)} %param.23) | copy-start | bytes 292
  0.0 8.7 %copy-start.9 = (bf16[4,1024]{1,0:T(4,128)(2,1)S(1)}, bf16[4,1024]{1,0:T(4,128)(2,1)}, u32[]{:S(2)}) copy-start(bf16[4,1024]{1,0:T(4,128)(2,1)} %taps_ref.2) | copy-start | bytes 24580
  0.0 8.7 %copy-start.8 = (f32[2048]{0:T(1024)S(1)}, f32[2048]{0:T(1024)}, u32[]{:S(2)}) copy-start(f32[2048]{0:T(1024)} %param.14) | copy-start | bytes 24580
  0.9 6.7 %collective-permute-start.2 = (bf16[16,2048]{1,0:T(8,128)(2,1)S(1)}, bf16[16,2048]{1,0:T(8,128)(2,1)S(1)}, u32[]{:S(2)}, u32[]{:S(2)}) collective-permute-start(bf16[16,2048]{1,0:T(8,128)(2,1)S(1)} %slice.9), channel_id=1, source_target_pairs={{1,3},{3,5},{5,7},{7,9},{9,11},{11,13},{13,15},{15,17},{17,19},{19... | collective-permute-start | bytes 196616 | tf_op jit(solution)/shard_map/ppermute | solution.py:354
  4.9 2.7 %collective-permute-start.1 = (bf16[16,2048]{1,0:T(8,128)(2,1)S(1)}, bf16[16,2048]{1,0:T(8,128)(2,1)S(1)}, u32[]{:S(2)}, u32[]{:S(2)}) collective-permute-start(bf16[16,2048]{1,0:T(8,128)(2,1)S(1)} %slice.9), channel_id=1, source_target_pairs={{1,2},{3,4},{5,6},{7,8},{9,10},{11,12},{13,14},{15,16},{17,18},{19... | collective-permute-start | bytes 196616 | tf_op jit(solution)/shard_map/ppermute | solution.py:355
  6.2 2.6 %collective-permute-start = (bf16[192,2048]{1,0:T(8,128)(2,1)}, bf16[192,2048]{1,0:T(8,128)(2,1)S(1)}, u32[]{:S(2)}, u32[]{:S(2)}) collective-permute-start(bf16[192,2048]{1,0:T(8,128)(2,1)} %own_ref.1), channel_id=1, source_target_pairs={{0,1},{1,0},{2,3},{3,2},{4,5},{5,4},{6,7},{7,6},{8,9},{9,8},{10,11... | collective-permute-start | bytes 2359304 | tf_op jit(solution)/shard_map/ppermute | solution.py:352
  8.8 20.0 %copy-start.10 = (bf16[4,1024]{1,0:T(4,128)(2,1)S(1)}, bf16[4,1024]{1,0:T(4,128)(2,1)}, u32[]{:S(2)}) copy-start(bf16[4,1024]{1,0:T(4,128)(2,1)} %taps_ref.3) | copy-start | bytes 24580
  17.8 22.0 %all-to-all-start = ((bf16[64,8,384]{2,1,0:T(8,128)(2,1)}), bf16[64,8,384]{2,1,0:T(8,128)(2,1)S(1)}, u32[]{:S(2)}, u32[]{:S(2)}) async-start(bf16[64,8,384]{2,1,0:T(8,128)(2,1)} %bitcast.2), calls=%async_computation | async-start | bytes 786432 | tf_op jit(solution)/shard_map/all_to_all | solution.py:382
  28.7 19.0 %copy-start.6 = (f32[2048]{0:T(1024)S(1)}, f32[2048]{0:T(1024)}, u32[]{:S(2)}) copy-start(f32[2048]{0:T(1024)} %param.24) | copy-start | bytes 24580
  42.1 16.2 %all-to-all-start.1 = ((bf16[64,8,384]{2,1,0:T(8,128)(2,1)}), bf16[64,8,384]{2,1,0:T(8,128)(2,1)S(1)}, u32[]{:S(2)}, u32[]{:S(2)}) async-start(bf16[64,8,384]{2,1,0:T(8,128)(2,1)} %shard_map.129), calls=%async_computation.1 | async-start | bytes 786432 | tf_op jit(solution)/shard_map/all_to_all | solution.py:402
  52.3 1.9 %copy-start = (bf16[1024,2048]{1,0:T(8,128)(2,1)}, bf16[1024,2048]{1,0:T(8,128)(2,1)S(1)}, u32[]{:S(2)}) copy-start(bf16[1024,2048]{1,0:T(8,128)(2,1)S(1)} %get-tuple-element.46.wout_ref) | copy-start | bytes 12582916
  54.3 0.7 %copy-start.2 = (bf16[384,512]{1,0:T(8,128)(2,1)}, bf16[384,512]{1,0:T(8,128)(2,1)S(1)}, u32[]{:S(2)}) copy-start(bf16[384,512]{1,0:T(8,128)(2,1)S(1)} %get-tuple-element.41.query_ref) | copy-start | bytes 1179652
  55.0 0.7 copy-start.4
  58.3 2.2 %copy-start.1 = (bf16[1024,2048]{1,0:T(8,128)(2,1)S(1)}, bf16[1024,2048]{1,0:T(8,128)(2,1)}, u32[]{:S(2)}) copy-start(bf16[1024,2048]{1,0:T(8,128)(2,1)} %copy-done) | copy-start | bytes 12582916
  60.5 1.0 %copy-start.3 = (bf16[384,512]{1,0:T(8,128)(2,1)S(1)}, bf16[384,512]{1,0:T(8,128)(2,1)}, u32[]{:S(2)}) copy-start(bf16[384,512]{1,0:T(8,128)(2,1)} %copy-done.2) | copy-start | bytes 1179652
  61.5 0.9 %copy-start.5 = (f32[384,128]{1,0:T(8,128)S(1)}, f32[384,128]{1,0:T(8,128)}, u32[]{:S(2)}) copy-start(f32[384,128]{1,0:T(8,128)} %copy-done.4) | copy-start | bytes 589828
  64.5 4.2 %collective-permute-start.3 = (bf16[192,2048]{1,0:T(8,128)(2,1)S(1)}, bf16[192,2048]{1,0:T(8,128)(2,1)S(1)}, u32[]{:S(2)}, u32[]{:S(2)}) collective-permute-start(bf16[192,2048]{1,0:T(8,128)(2,1)S(1)} %shard_map.132), channel_id=1, source_target_pairs={{0,1},{1,0},{2,3},{3,2},{4,5},{5,4},{6,7},{7,6},{8,9},{9,8},{10,11... | collective-permute-start | bytes 2359304 | tf_op jit(solution)/shard_map/ppermute | solution.py:416

commit v3 on v2

--- a/solution.py
+++ b/solution.py
@@ -77,38 +77,42 @@
     return acc * (1.0 / (1.0 + jnp.exp(-acc)))
 
 
-def summary_kernel(own_ref, oth_ref, one_ref, two_ref, gain_ref, wk_hbm, wv_hbm, wg_ref, taps_ref, offs_ref,
-                   key_out, value_out, logs_out, piece_ref, rows_out,
-                   key_ref, value_ref, logs_ref, rows_ref, wk_ref, wv_ref, pre_ref, sems, out_sems):
+def normalized(x, gain):
+    x = x.astype(F32)
+    scale = lax.rsqrt(jnp.mean(x * x, axis=-1, keepdims=True) + EPS)
+    return (x * scale * gain).astype(BF)
+
+
+def fetch_kernel(own_ref, gain_ref, wk_hbm, wv_hbm, rows_ref, wk_ref, wv_ref, sems):
     wide = HEADS * DV // 2
     copies = started(
         [(wk_hbm, wk_ref)]
         + [(wv_hbm.at[:, pl.ds(c * wide, wide)], wv_ref.at[:, pl.ds(c * wide, wide)]) for c in range(2)],
         sems,
     )
+    gain = gain_ref[...]
+    for part in range(HALF // 48):
+        rows_ref[part * 48 : part * 48 + 48, :] = normalized(own_ref[part * 48 : part * 48 + 48, :], gain)
+    for copy in copies:
+        copy.wait()
+
+
+def summary_kernel(own_ref, oth_ref, one_ref, two_ref, gain_ref, wk_ref, wv_ref, wg_ref, taps_ref, offs_ref,
+                   key_out, value_out, logs_out, piece_ref, rows_ref, pre_ref, key_ref, value_ref, logs_ref, sems):
     outs = [
-        pltpu.make_async_copy(src, dst, out_sems.at[n])
-        for n, (src, dst) in enumerate(
-            [(rows_ref, rows_out), (logs_ref, logs_out), (key_ref, key_out), (value_ref, value_out)]
-        )
+        pltpu.make_async_copy(src, dst, sems.at[n])
+        for n, (src, dst) in enumerate([(logs_ref, logs_out), (key_ref, key_out), (value_ref, value_out)])
     ]
     tp = lax.axis_index("tp")
     gain = gain_ref[...]
-
-    def normalized(x):
-        x = x.astype(F32)
-        scale = lax.rsqrt(jnp.mean(x * x, axis=-1, keepdims=True) + EPS)
-        return (x * scale * gain).astype(BF)
-
-    rows_ref[0:TAIL, :] = normalized(one_ref[...] + two_ref[...])
-    for ref, at in ((own_ref, tp), (oth_ref, 1 - tp)):
-        for part in range(HALF // 48):
-            to = pl.multiple_of(TAIL + at * HALF + part * 48, 16)
-            rows_ref[pl.ds(to, 48), :] = normalized(ref[part * 48 : part * 48 + 48, :])
-    outs[0].start()
+    rows_ref[0:TAIL, :] = normalized(one_ref[...] + two_ref[...], gain)
+    mine = pl.multiple_of(TAIL + tp * HALF, 16)
+    rows_ref[pl.ds(mine, HALF), :] = own_ref[...]
+    for part in range(HALF // 48):
+        to = pl.multiple_of(TAIL + (1 - tp) * HALF + part * 48, 16)
+        rows_ref[pl.ds(to, 48), :] = normalized(oth_ref[part * 48 : part * 48 + 48, :], gain)
     own = pl.ds(TAIL, ROWS)
     gates = jnp.dot(rows_ref[own, :], wg_ref[...], preferred_element_type=F32)
-    copies[0].wait()
     pre_ref[...] = jnp.dot(rows_ref[...], wk_ref[...], preferred_element_type=F32).astype(BF).astype(F32)
 
     lane = lane_of((SPAN, 128))
@@ -123,7 +127,7 @@
         gate.append(g)
         inside.append(total)
         totals.append(total[SPAN - 1 : SPAN, :])
-    outs[1].start()
+    outs[0].start()
     write, level = [], None
     later = jnp.zeros_like(totals[0])
     for b in reversed(range(BLOCKS)):
@@ -141,12 +145,9 @@
         for b in range(BLOCKS):
             rows = slice(b * SPAN, (b + 1) * SPAN)
             key_ref[rows, lanes] = (mixed_rows(pre_ref, taps, lanes, b * SPAN, SPAN) * DQK**-0.5).astype(BF)
+    outs[1].start()
+    value_ref[...] = jnp.dot(rows_ref[own, :], wv_ref[...], preferred_element_type=F32).astype(BF)
     outs[2].start()
-    for c in range(2):
-        copies[1 + c].wait()
-        cols = slice(c * wide, (c + 1) * wide)
-        value_ref[:, cols] = jnp.dot(rows_ref[own, :], wv_ref[:, cols], preferred_element_type=F32).astype(BF)
-    outs[3].start()
     ones = jnp.ones((ROWS, 128), BF)
     dims = (((0,), (0,)), ((), ()))
     for h in range(HEADS):
@@ -169,56 +170,62 @@
         copy.wait()
 
 
-def prefix_kernel(piece_ref, out_ref, wide_ref, done_ref):
-    count = piece_ref.shape[0]
-    wide_ref[...] = piece_ref[...].astype(F32)
-    extra = wide_ref[:, 0, DV:]
+def prefix_kernel(piece_ref, out_ref):
+    count = piece_ref.shape[0] // 8
+    tall = piece_ref.shape[0]
+
+    def iota(shape, dim):
+        return lax.broadcasted_iota(jnp.int32, shape, dim)
+
+    def ones_where(test):
+        return jnp.where(test, 1.0, 0.0).astype(BF)
+
+    first = ones_where(iota((count, tall), 1) == 8 * iota((count, tall), 0))
+    down = iota((tall, count), 0) - 8 * iota((tall, count), 1)
+    spread = ones_where((down >= 0) & (down < 8))
+    over = iota((count, tall), 1) - 8 * iota((count, tall), 0)
+    spread_over = ones_where((over >= 0) & (over < 8))
+    extra = jnp.dot(first, piece_ref[:, DV:], preferred_element_type=F32)
     lane = lane_of((count, 128))
 
-    def number(first):
-        return jnp.sum(jnp.where((lane >= first) & (lane < first + 3), extra, 0.0), axis=1, keepdims=True)
+    def number(at):
+        return jnp.sum(jnp.where((lane >= at) & (lane < at + 3), extra, 0.0), axis=1, keepdims=True)
 
     forget, level = number(1), number(4)
-    down = lax.broadcasted_iota(jnp.int32, (count, count), 0)
-    over = lax.broadcasted_iota(jnp.int32, (count, count), 1)
+    down, over = iota((count, count), 0), iota((count, count), 1)
     steps = jnp.where(down > over, forget, jnp.where(down == over, level, 0.0))
     earlier = over < down
-    logs = jnp.dot(earlier.astype(F32), steps, precision=HIGHEST, preferred_element_type=F32)
+    logs = jnp.dot(jnp.where(earlier, 1.0, 0.0), steps, precision=HIGHEST, preferred_element_type=F32)
     logs = jnp.where(earlier, logs, EMPTY)
     top = jnp.max(logs, axis=1, keepdims=True)
-    weight = jnp.where(earlier, jnp.exp(logs - top), 0.0)
-    high = weight.astype(BF)
-    low = (weight - high.astype(F32)).astype(BF)
-    marks = thirds(top)
-    lane = lane_of((count, WIDTH))
-    for r in range(8):
-        part = wide_ref[:, r, :].astype(BF)
-        state = jnp.dot(high, part, preferred_element_type=F32) + jnp.dot(low, part, preferred_element_type=F32)
-        for n, mark in enumerate(marks):
-            state = jnp.where(lane == DV + 1 + n, mark, state)
-        done_ref[:, r, :] = state
-    out_ref[...] = done_ref[...].astype(BF)
-
-
-def local_kernel(rows_hbm, wq_hbm, key_hbm, value_hbm, logs_hbm, taps_ref,
-                 query_out, numer_out, stats_out,
-                 rows_ref, wq_ref, key_ref, value_ref, logs_ref, pre_ref, query_ref, numer_ref, stats_ref, sems, out_sems):
-    copies = started(
-        [(rows_hbm, rows_ref), (wq_hbm, wq_ref), (logs_hbm, logs_ref), (key_hbm, key_ref), (value_hbm, value_ref)], sems
-    )
+    weight = jnp.where(earlier, jnp.exp(logs - top), 0.0).astype(BF)
+    weight = jnp.dot(weight, spread_over, preferred_element_type=F32).astype(BF)
+    weight = jnp.dot(spread, weight, preferred_element_type=F32)
+    same = (iota((tall, tall), 0) & 7) == (iota((tall, tall), 1) & 7)
+    weight = jnp.where(same, weight, 0.0).astype(BF)
+    marks = jnp.zeros((count, 128), F32)
+    for n, mark in enumerate(thirds(top)):
+        marks = jnp.where(lane == n + 1, mark, marks)
+    marks = jnp.dot(spread, marks.astype(BF), preferred_element_type=F32)
+    state = jnp.dot(weight, piece_ref[...], preferred_element_type=F32)
+    lane = lane_of((tall, 128))
+    out_ref[:, :DV] = state[:, :DV].astype(BF)
+    out_ref[:, DV:] = jnp.where((lane >= 1) & (lane < 4), marks, state[:, DV:]).astype(BF)
+
+
+def local_kernel(rows_ref, wq_hbm, key_hbm, value_hbm, logs_hbm, taps_ref,
+                 query_ref, numer_ref, stats_ref, wq_ref, pre_ref, key_ref, value_ref, logs_ref, sems):
+    copies = started([(wq_hbm, wq_ref), (logs_hbm, logs_ref), (key_hbm, key_ref), (value_hbm, value_ref)], sems)
     tp = lax.axis_index("tp")
     taps = taps_ref[:, pl.ds(pl.multiple_of(tp * (HEADS * DQK), 128), HEADS * DQK)].astype(F32)
     copies[0].wait()
-    copies[1].wait()
     pre_ref[...] = jnp.dot(rows_ref[...], wq_ref[...], preferred_element_type=F32).astype(BF).astype(F32)
     for h in range(HEADS):
         lanes = slice(h * DQK, (h + 1) * DQK)
         for b in range(BLOCKS):
             rows = slice(b * SPAN, (b + 1) * SPAN)
             query_ref[rows, lanes] = mixed_rows(pre_ref, taps, lanes, b * SPAN, SPAN).astype(BF)
-    outs = [pltpu.make_async_copy(query_ref, query_out, out_sems.at[0])]
-    outs[0].start()
-    for copy in copies[2:]:
+    for copy in copies[1:]:
         copy.wait()
     lane = lane_of((SPAN, 128))
     cols = [logs_ref[b * SPAN : (b + 1) * SPAN, :] for b in range(BLOCKS)]
@@ -259,41 +266,26 @@
                 lax.dot_general(query_ref[rows, head], key_ref[:seen, head], nt, preferred_element_type=F32) * weight
             )
             denom = jnp.sum(scores, axis=1, keepdims=True)
-            numer_ref[rows, wide] = jnp.dot(scores.astype(BF), value_ref[:seen, wide], preferred_element_type=F32)
+            numer = jnp.dot(scores.astype(BF), value_ref[:seen, wide], preferred_element_type=F32)
+            numer_ref[rows, wide] = numer.astype(BF)
             stats[t] = jnp.where(lane == h, denom, jnp.where(lane == HEADS + h, top, stats[t]))
-        outs.append(
-            pltpu.make_async_copy(
-                numer_ref.at[:, pl.ds(h * DV, DV)], numer_out.at[:, pl.ds(h * DV, DV)], out_sems.at[1 + h]
-            )
-        )
-        outs[-1].start()
     for t in range(BLOCKS):
         stats_ref[t * SPAN : (t + 1) * SPAN, :] = stats[t]
-    outs.append(pltpu.make_async_copy(stats_ref, stats_out, out_sems.at[1 + HEADS]))
-    outs[-1].start()
-    for copy in outs:
-        copy.wait()
-
-
-def gate_kernel(rows_hbm, wo_hbm, gain_ref, query_hbm, numer_hbm, stats_hbm, wout_hbm,
-                ogate_ref, query_ref, numer_ref, stats_ref, wout_ref, rows_ref, wo_ref, sems):
-    wide = HEADS * DV // 2
+
+
+def gate_kernel(rows_ref, wo_hbm, gain_ref, ogate_ref, wo_ref, sems):
+    wide = HEADS * DV // 4
     copies = started(
-        [(rows_hbm, rows_ref)]
-        + [(wo_hbm.at[:, pl.ds(c * wide, wide)], wo_ref.at[:, pl.ds(c * wide, wide)]) for c in range(2)]
-        + [(query_hbm, query_ref), (numer_hbm, numer_ref), (stats_hbm, stats_ref), (wout_hbm, wout_ref)],
+        [(wo_hbm.at[:, pl.ds(c * wide, wide)], wo_ref.at[:, pl.ds(c * wide, wide)]) for c in range(4)],
         sems,
     )
     tp = lax.axis_index("tp")
     gain = gain_ref[:, pl.ds(pl.multiple_of(tp * (HEADS * DV), 128), HEADS * DV)]
-    copies[0].wait()
-    for c in range(2):
-        copies[1 + c].wait()
+    for c in range(4):
+        copies[c].wait()
         cols = slice(c * wide, (c + 1) * wide)
         pre = jnp.dot(rows_ref[pl.ds(TAIL, ROWS), :], wo_ref[:, cols], preferred_element_type=F32).astype(BF).astype(F32)
-        ogate_ref[:, cols] = gain[:, cols] / (1.0 + jnp.exp(-pre))
-    for copy in copies[3:]:
-        copy.wait()
+        ogate_ref[:, cols] = (gain[:, cols] / (1.0 + jnp.exp(-pre))).astype(BF)
 
 
 def hidden_rows(first, query_ref, ogate_ref, state_ref, numer_ref, stats_ref, hidden_ref):
@@ -324,15 +316,22 @@
         read = jnp.dot(
             query[:, h * DQK : (h + 1) * DQK], state_ref[h * DQK : (h + 1) * DQK, :DV], preferred_element_type=F32
         )
-        cell = one[:, h : h + 1] * read + two[:, h : h + 1] * numer_ref[rows, wide]
+        cell = one[:, h : h + 1] * read + two[:, h : h + 1] * numer_ref[rows, wide].astype(F32)
         scale = lax.rsqrt(jnp.mean(cell * cell, axis=-1, keepdims=True) + EPS)
-        hidden_ref[:, wide] = (cell * scale * ogate_ref[rows, wide]).astype(BF)
-
-
-def sent_kernel(query_ref, ogate_ref, state_ref, numer_ref, stats_ref, wout_ref, out_ref, hidden_ref):
+        hidden_ref[:, wide] = (cell * scale * ogate_ref[rows, wide].astype(F32)).astype(BF)
+
+
+def sent_kernel(query_ref, ogate_ref, state_ref, numer_ref, stats_ref, wout_hbm, out_ref, wout_ref, hidden_ref, sems):
+    deep = HEADS * DV // 2
+    copies = started(
+        [(wout_hbm.at[pl.ds(c * deep, deep)], wout_ref.at[pl.ds(c * deep, deep)]) for c in range(2)], sems
+    )
     first = (1 - lax.axis_index("tp")) * HALF
     hidden_rows(first, query_ref, ogate_ref, state_ref, numer_ref, stats_ref, hidden_ref)
-    out_ref[...] = jnp.dot(hidden_ref[...], wout_ref[...], preferred_element_type=F32).astype(BF)
+    copies[0].wait()
+    part = jnp.dot(hidden_ref[:, :deep], wout_ref[:deep, :], preferred_element_type=F32)
+    copies[1].wait()
+    out_ref[...] = (part + jnp.dot(hidden_ref[:, deep:], wout_ref[deep:, :], preferred_element_type=F32)).astype(BF)
 
 
 def kept_kernel(query_ref, ogate_ref, state_ref, numer_ref, stats_ref, wout_ref, out_ref, hidden_ref):
@@ -370,52 +369,51 @@
     def room(like):
         return pltpu.VMEM(like.shape, like.dtype)
 
+    own, wk, wv = call(
+        fetch_kernel,
+        (shape(tokens.shape, BF), shape(w_key.shape, BF), shape(w_value.shape, BF)),
+        (v, v, v),
+        [n, n, m, m],
+        [dma((3,))],
+        flops=1_000_000_000,
+    )(tokens, gain, w_key, w_value)
     key, value, logs, pieces, rows = call(
         summary_kernel,
         (key_shape, value_shape, logs_shape, shape((HEADS * DQK, WIDTH), BF), rows_shape),
-        (m, m, m, n, m),
-        [n, n, n, n, n, m, m, n, n, n],
-        [room(key_shape), room(value_shape), room(logs_shape), room(rows_shape), room(w_key), room(w_value), room(pre_shape), dma((3,)), dma((4,))],
+        (m, m, m, n, v),
+        [v, n, n, n, n, v, v, n, n, n],
+        [room(pre_shape), room(key_shape), room(value_shape), room(logs_shape), dma((3,))],
         flops=3_000_000_000,
-        limit=20,
-    )(tokens, other, to_first, to_second, gain, w_key, w_value, w_gates, conv_key, offsets)
+    )(own, other, to_first, to_second, gain, wk, wv, w_gates, conv_key, offsets)
     pieces = lax.all_to_all(pieces.reshape(stretches, 8, WIDTH), SP, 0, 0, tiled=True)
     query, numer, stats = call(
         local_kernel,
-        (key_shape, wide_shape, logs_shape),
-        (m, m, m),
-        [m, m, m, m, m, n],
-        [room(rows_shape), room(w_query), room(key_shape), room(value_shape), room(logs_shape), room(pre_shape), room(key_shape), room(wide_shape), room(logs_shape), dma((5,)), dma((2 + HEADS,))],
+        (key_shape, value_shape, logs_shape),
+        (v, v, v),
+        [v, m, m, m, m, n],
+        [room(w_query), room(pre_shape), room(key_shape), room(value_shape), room(logs_shape), dma((4,))],
         flops=3_000_000_000,
-        limit=16,
     )(rows, w_query, key, value, logs, conv_query)
     pieces, query, numer, stats = lax.optimization_barrier((pieces, query, numer, stats))
-    state = call(
-        prefix_kernel,
-        shape((stretches, 8, WIDTH), BF),
-        n,
-        [n],
-        [pltpu.VMEM((stretches, 8, WIDTH), F32), pltpu.VMEM((stretches, 8, WIDTH), F32)],
-        flops=100_000_000,
-    )(pieces)
-    state, query, numer, stats = lax.optimization_barrier((state, query, numer, stats))
-    state = lax.all_to_all(state, SP, 0, 0, tiled=True).reshape(HEADS * DQK, WIDTH)
-    ogate, query, numer, stats, w_last = call(
-        gate_kernel,
-        (wide_shape, key_shape, wide_shape, logs_shape, shape(w_out.shape, BF)),
-        (v, v, v, v, v),
-        [m, m, n, m, m, m, m],
-        [room(rows_shape), room(w_ogate), dma((7,))],
-        flops=3_000_000_000,
-        limit=10,
-    )(rows, w_ogate, head_gain, query, numer, stats, w_out)
+    piece_shape = shape((stretches * 8, WIDTH), BF)
+    state = call(prefix_kernel, piece_shape, n, [n], flops=100_000_000)(pieces.reshape(piece_shape.shape))
+    state, query, numer, stats, rows = lax.optimization_barrier((state, query, numer, stats, rows))
+    state = lax.all_to_all(state.reshape(stretches, 8, WIDTH), SP, 0, 0, tiled=True).reshape(HEADS * DQK, WIDTH)
+    ogate = call(
+        gate_kernel, value_shape, v, [v, m, n], [room(w_ogate), dma((4,))], flops=3_000_000_000
+    )(rows, w_ogate, head_gain)
     hidden = pltpu.VMEM((HALF, HEADS * DV), BF)
-    sent = call(sent_kernel, shape((HALF, width), BF), n, [v, v, n, v, v, v], [hidden], flops=1_000_000_000, limit=8)(
-        query, ogate, state, numer, stats, w_last
-    )
+    sent, wout = call(
+        sent_kernel,
+        (shape((HALF, width), BF), shape(w_out.shape, BF)),
+        (n, v),
+        [v, v, n, v, v, m],
+        [hidden, dma((2,))],
+        flops=1_000_000_000,
+    )(query, ogate, state, numer, stats, w_out)
     got = lax.ppermute(sent, "tp", [(0, 1), (1, 0)])
-    kept = call(kept_kernel, shape((HALF, width), F32), n, [v, v, n, v, v, v], [hidden], flops=1_000_000_000, limit=8)(
-        query, ogate, state, numer, stats, w_last
+    kept = call(kept_kernel, shape((HALF, width), F32), n, [v, v, n, v, v, v], [hidden], flops=1_000_000_000)(
+        query, ogate, state, numer, stats, wout
     )
     return (kept + got.astype(F32)).astype(BF)
 

time: 70.3 us -> 69.2 us (0.984)
  local copies, waits for them, and re-layouts: 9.6 us -> 7.62 us
    unnamed x25 -> x19, local copies, waits for them, and re-layouts: 7.51 us -> 4.76 us
    ppermute x1, waiting for transfers between devices: 1.14 us -> 0.01 us  [body(): other = lax.ppermute(tokens, 'tp', [(0, 1), (1, 0)])]
    all_to_all x1, waiting for transfers between devices: 2.65 us -> 3.63 us  [body(): lax.all_to_all(state.reshape(stretches, 8, WIDTH), SP, 0, 0, tiled=True)]
    slice x1, local copies, waits for them, and re-layouts: 0.01 us -> 0.77 us  [body(): offsets = jnp.concatenate([gate_offset[0], gate_offset[1]], axis=1)]
    pallas_call x6 -> x7, Pallas kernels: 26.7 us -> 27.4 us  [call(): return lambda *args: run(*map(kept, args, spaces))]
  transfers between devices with their start and end apart: 6 -> 6, of which waited for: 3 -> 2; matrix products, arithmetic and copies ran while one was open for 2% -> 3% of each run, Pallas kernels for 19% -> 23%
where the time goes in v3:
time: 69.2 us; the launch traced here: 68.7 us
  Pallas kernels  27.4 us (40%)
  starting transfers between devices  24.6 us (36%)
  waiting for transfers between devices  7.74 us (11%)
  local copies, waits for them, and re-layouts  7.62 us (11%)
  other arithmetic  1.19 us (2%)
    pallas_call x7, Pallas kernels, call(): return lambda *args: run(*map(kept, args, spaces))  27.4 us
    all_to_all x1, starting transfers between devices, body(): lax.all_to_all(pieces.reshape(stretches, 8, WIDTH), SP, 0, 0, tiled=True)  10.8 us
    all_to_all x1, starting transfers between devices, body(): lax.all_to_all(state.reshape(stretches, 8, WIDTH), SP, 0, 0, tiled=True)  5.87 us
    unnamed x19, local copies, waits for them, and re-layouts  4.76 us
    all_to_all x1, waiting for transfers between devices, body(): lax.all_to_all(pieces.reshape(stretches, 8, WIDTH), SP, 0, 0, tiled=True)  4.1 us
    ppermute x1, starting transfers between devices, body(): lax.ppermute(last, SP_TP, [(2 * i + 1, 2 * i + 3) for i in range(stretche...  3.92 us
    all_to_all x1, waiting for transfers between devices, body(): lax.all_to_all(state.reshape(stretches, 8, WIDTH), SP, 0, 0, tiled=True)  3.63 us
    ppermute x1, starting transfers between devices, body(): got = lax.ppermute(sent, 'tp', [(0, 1), (1, 0)])  2.56 us
  transfers between devices with their start and end apart: 6, of which 2 were waited for; matrix products, arithmetic and copies ran while one was open for 3% of the time, Pallas kernels for 23%

profile of v3, /device:TPU:1, one launch (start us, length us, event | category | flops | bytes accessed | tf_op | source)
XLA Modules:
  0.0 68.7 jit_solution(2674110224232979076)
XLA Ops:
  0.0 0.0 copy-start
  0.0 0.9 %slice.9 = bf16[16,2048]{1,0:T(8,128)(2,1)S(1)} slice(bf16[192,2048]{1,0:T(8,128)(2,1)} %own_ref.1), slice={[176:192], [0:2048]} | slice | bytes 131072 | tf_op jit(solution)/shard_map/slice | solution.py:352
  0.9 3.9 %collective-permute-start.2 = (bf16[16,2048]{1,0:T(8,128)(2,1)S(1)}, bf16[16,2048]{1,0:T(8,128)(2,1)S(1)}, u32[]{:S(2)}, u32[]{:S(2)}) collective-permute-start(bf16[16,2048]{1,0:T(8,128)(2,1)S(1)} %slice.9), channel_id=1, source_target_pairs={{1,3},{3,5},{5,7},{7,9},{9,11},{11,13},{13,15},{15,17},{17,19},{19... | collective-permute-start | bytes 196616 | tf_op jit(solution)/shard_map/ppermute | solution.py:353
  4.9 1.3 %collective-permute-start.1 = (bf16[16,2048]{1,0:T(8,128)(2,1)S(1)}, bf16[16,2048]{1,0:T(8,128)(2,1)S(1)}, u32[]{:S(2)}, u32[]{:S(2)}) collective-permute-start(bf16[16,2048]{1,0:T(8,128)(2,1)S(1)} %slice.9), channel_id=1, source_target_pairs={{1,2},{3,4},{5,6},{7,8},{9,10},{11,12},{13,14},{15,16},{17,18},{19... | collective-permute-start | bytes 196616 | tf_op jit(solution)/shard_map/ppermute | solution.py:354
  6.2 0.1 collective-permute-start
  6.3 0.8 %constant_dynamic-slice_fusion = (bf16[2048,4]{0,1:T(4,128)(2,1)S(1)}, bf16[2048,4]{0,1:T(4,128)(2,1)S(1)}) fusion(bf16[2048,8]{0,1:T(8,128)(2,1)} %param.20, s32[]{:T(128)S(6)} %select_n.4, bf16[2048,8]{0,1:T(8,128)(2,1)} %param.19), kind=kLoop, calls=%fused_computation.6 | loop fusion | bytes 65540 | tf_op jit(solution)/shard_map/dynamic_slice | solution.py:356
  7.1 0.3 copy.18
  7.4 0.1 pad.8.wg_ref
  7.5 0.8 %fusion = (f32[1,3,4]{2,0,1:T(1,128)S(1)}, f32[1,3,4]{2,0,1:T(1,128)S(1)}) fusion(f32[2,3,4]{2,0,1:T(2,128)} %param.23), kind=kLoop, calls=%fused_computation.8 | loop fusion | bytes 192 | tf_op jit(solution)/shard_map/slice | solution.py:359
  8.2 0.1 select_maximum_fusion.offs_ref
  8.3 0.0 copy-done
  8.3 0.0 copy-start.1
  8.3 0.7 %copy-done.1 = f32[2048]{0:T(1024)S(1)} copy-done((f32[2048]{0:T(1024)S(1)}, f32[2048]{0:T(1024)}, u32[]{:S(2)}) %copy-start.1) | copy-done | bytes 8216
  9.0 0.0 copy-start.2
  9.0 0.0 copy-start.3
  9.0 2.9 %shard_map.127 = (bf16[192,2048]{1,0:T(8,128)(2,1)S(1)}, bf16[2048,512]{1,0:T(8,128)(2,1)S(1)}, bf16[2048,1024]{1,0:T(8,128)(2,1)S(1)}) custom-call(bf16[192,2048]{1,0:T(8,128)(2,1)S(1)} %copy-done, f32[1,2048]{1,0:T(1,128)S(1)} %bitcast.13, bf16[2048,512]{1,0:T(8,128)(2,1)} %wk_hbm.1, bf16[2048,1024]{1,0:T(8,128)(2,1)} %wv_hbm.1), custom_call_target="tpu_custom_call" | custom-call | flops 1000000000 | bytes 1048576 | tf_op jit(solution)/shard_map/pallas_call | solution.py:51
  11.9 0.0 collective-permute-done.2.two_ref
  12.0 0.0 collective-permute-done.1.one_ref
  12.0 0.0 collective-permute-done.oth_ref
  12.0 0.0 copy-done.2
  12.0 0.0 copy-done.3
  12.0 0.0 copy-start.4
  12.0 5.9 %shard_map.128 = (bf16[384,512]{1,0:T(8,128)(2,1)}, bf16[384,1024]{1,0:T(8,128)(2,1)}, f32[384,128]{1,0:T(8,128)}, bf16[512,384]{1,0:T(8,128)(2,1)}, bf16[400,2048]{1,0:T(8,128)(2,1)S(1)}) custom-call(bf16[192,2048]{1,0:T(8,128)(2,1)S(1)} %get-tuple-element.27.own_ref, bf16[192,2048]{1,0:T(8,128)(2,1)S(1)} %collective-permute-done.oth_ref, ...), custom_call_target="tpu_custom_call" | custom-call | flops 3000000000 | bytes 1048576 | tf_op jit(solution)/shard_map/pallas_call | solution.py:51
  17.9 0.0 copy-start.6
  17.9 1.2 %copy-done.6 = bf16[400,2048]{1,0:T(8,128)(2,1)} copy-done((bf16[400,2048]{1,0:T(8,128)(2,1)}, bf16[400,2048]{1,0:T(8,128)(2,1)S(1)}, u32[]{:S(2)}) %copy-start.6) | copy-done | bytes 1638424
  19.1 10.8 %all-to-all-start = ((bf16[64,8,384]{2,1,0:T(8,128)(2,1)}), bf16[64,8,384]{2,1,0:T(8,128)(2,1)S(1)}, u32[]{:S(2)}, u32[]{:S(2)}) async-start(bf16[64,8,384]{2,1,0:T(8,128)(2,1)} %bitcast.1), calls=%async_computation | async-start | bytes 786432 | tf_op jit(solution)/shard_map/all_to_all | solution.py:388
  30.0 0.0 copy-done.4
  30.0 0.0 copy-start.7
  30.0 1.4 %copy-done.7 = bf16[400,2048]{1,0:T(8,128)(2,1)S(1)} copy-done((bf16[400,2048]{1,0:T(8,128)(2,1)S(1)}, bf16[400,2048]{1,0:T(8,128)(2,1)}, u32[]{:S(2)}) %copy-start.7) | copy-done | bytes 1638424
  31.4 0.0 copy-start.5
  31.4 5.4 %shard_map.129 = (bf16[384,512]{1,0:T(8,128)(2,1)S(1)}, bf16[384,1024]{1,0:T(8,128)(2,1)S(1)}, f32[384,128]{1,0:T(8,128)S(1)}) custom-call(bf16[400,2048]{1,0:T(8,128)(2,1)S(1)} %copy-done.7, bf16[2048,512]{1,0:T(8,128)(2,1)} %wq_hbm.1, bf16[384,512]{1,0:T(8,128)(2,1)} %get-tuple-element.32.key_hbm, bf16[384,1024]{1,0:T(8,128)(2,1)} %get-tuple-element.33.value_hbm, ...), custom_call_target="tpu_custom_call" | custom-call | flops 3000000000 | bytes 1048576 | tf_op jit(solution)/shard_map/pallas_call | solution.py:51
  36.8 4.1 %all-to-all-done = bf16[64,8,384]{2,1,0:T(8,128)(2,1)S(1)} async-done(((bf16[64,8,384]{2,1,0:T(8,128)(2,1)}), bf16[64,8,384]{2,1,0:T(8,128)(2,1)S(1)}, u32[]{:S(2)}, u32[]{:S(2)}) %all-to-all-start) | async-done | bytes 393248 | tf_op jit(solution)/shard_map/all_to_all | solution.py:388
  40.9 2.0 %shard_map.130 = bf16[512,384]{1,0:T(8,128)(2,1)} custom-call(bf16[512,384]{1,0:T(8,128)(2,1)S(1)} %bitcast.12), custom_call_target="tpu_custom_call" | custom-call | flops 100000000 | bytes 1048576 | tf_op jit(solution)/shard_map/pallas_call | solution.py:51
  42.9 5.9 %all-to-all-start.1 = ((bf16[64,8,384]{2,1,0:T(8,128)(2,1)}), bf16[64,8,384]{2,1,0:T(8,128)(2,1)S(1)}, u32[]{:S(2)}, u32[]{:S(2)}) async-start(bf16[64,8,384]{2,1,0:T(8,128)(2,1)} %bitcast.4), calls=%async_computation.1 | async-start | bytes 786432 | tf_op jit(solution)/shard_map/all_to_all | solution.py:401
  48.8 0.0 copy-done.5
  48.8 0.0 copy-start.8
  48.8 1.4 %copy-done.8 = bf16[400,2048]{1,0:T(8,128)(2,1)S(1)} copy-done((bf16[400,2048]{1,0:T(8,128)(2,1)S(1)}, bf16[400,2048]{1,0:T(8,128)(2,1)}, u32[]{:S(2)}) %copy-start.8) | copy-done | bytes 1638424
  50.2 5.2 %shard_map.131.ogate_ref = bf16[384,1024]{1,0:T(8,128)(2,1)S(1)} custom-call(bf16[400,2048]{1,0:T(8,128)(2,1)S(1)} %copy-done.8, bf16[2048,1024]{1,0:T(8,128)(2,1)} %wo_hbm.1, f32[1,2048]{1,0:T(1,128)S(1)} %bitcast.15), custom_call_target="tpu_custom_call" | custom-call | flops 3000000000 | bytes 1048576 | tf_op jit(solution)/shard_map/pallas_call | solution.py:51
  55.4 3.6 %all-to-all-done.1 = bf16[64,8,384]{2,1,0:T(8,128)(2,1)S(1)} async-done(((bf16[64,8,384]{2,1,0:T(8,128)(2,1)}), bf16[64,8,384]{2,1,0:T(8,128)(2,1)S(1)}, u32[]{:S(2)}, u32[]{:S(2)}) %all-to-all-start.1) | async-done | bytes 393248 | tf_op jit(solution)/shard_map/all_to_all | solution.py:401
  59.0 4.0 %shard_map.132 = (bf16[192,2048]{1,0:T(8,128)(2,1)S(1)}, bf16[1024,2048]{1,0:T(8,128)(2,1)S(1)}) custom-call(bf16[384,512]{1,0:T(8,128)(2,1)S(1)} %get-tuple-element.42.query_ref, bf16[384,1024]{1,0:T(8,128)(2,1)S(1)} %shard_map.131.ogate_ref, bf16[512,384]{1,0:T(8,128)(2,1)S(1)} %bitcast.10, bf16[384,1024]{1,0:T(8,128)(2,1)S(1)} %get-tuple-element.45.numer_ref, ...), custom_call_target="tpu_custom_call" | custom-call | flops 1000000000 | bytes 1048576 | tf_op jit(solution)/shard_map/pallas_call | solution.py:51
  63.0 2.6 %collective-permute-start.3 = (bf16[192,2048]{1,0:T(8,128)(2,1)S(1)}, bf16[192,2048]{1,0:T(8,128)(2,1)S(1)}, u32[]{:S(2)}, u32[]{:S(2)}) collective-permute-start(bf16[192,2048]{1,0:T(8,128)(2,1)S(1)} %get-tuple-element.48), channel_id=1, source_target_pairs={{0,1},{1,0},{2,3},{3,2},{4,5},{5,4},{6,7},{7,6},{8,9},{9,8},{10,11... | collective-permute-start | bytes 2359304 | tf_op jit(solution)/shard_map/ppermute | solution.py:414
  65.6 2.0 %shard_map.133 = f32[192,2048]{1,0:T(8,128)S(1)} custom-call(bf16[384,512]{1,0:T(8,128)(2,1)S(1)} %get-tuple-element.42.query_ref, bf16[384,1024]{1,0:T(8,128)(2,1)S(1)} %shard_map.131.ogate_ref, bf16[512,384]{1,0:T(8,128)(2,1)S(1)} %bitcast.11, bf16[384,1024]{1,0:T(8,128)(2,1)S(1)} %get-tuple-element.45.numer_ref, ...), custom_call_target="tpu_custom_call" | custom-call | flops 1000000000 | bytes 1048576 | tf_op jit(solution)/shard_map/pallas_call | solution.py:51
  67.6 0.0 collective-permute-done.3
  67.6 1.1 %add_convert_fusion = bf16[192,2048]{1,0:T(8,128)(2,1)} fusion(f32[192,2048]{1,0:T(8,128)S(1)} %shard_map.133, bf16[192,2048]{1,0:T(8,128)(2,1)S(1)} %collective-permute-done.3), kind=kLoop, calls=%fused_computation | loop fusion | flops 1179648 | bytes 3145728 | tf_op jit(solution)/shard_map/convert_element_type | solution.py:418
  (2 shorter events, 0.0 us)
Async XLA Ops:
  0.0 8.3 %copy-start = (bf16[192,2048]{1,0:T(8,128)(2,1)S(1)}, bf16[192,2048]{1,0:T(8,128)(2,1)}, u32[]{:S(2)}) copy-start(bf16[192,2048]{1,0:T(8,128)(2,1)} %own_ref.1) | copy-start | bytes 2359300
  0.9 11.0 %collective-permute-start.2 = (bf16[16,2048]{1,0:T(8,128)(2,1)S(1)}, bf16[16,2048]{1,0:T(8,128)(2,1)S(1)}, u32[]{:S(2)}, u32[]{:S(2)}) collective-permute-start(bf16[16,2048]{1,0:T(8,128)(2,1)S(1)} %slice.9), channel_id=1, source_target_pairs={{1,3},{3,5},{5,7},{7,9},{9,11},{11,13},{13,15},{15,17},{17,19},{19... | collective-permute-start | bytes 196616 | tf_op jit(solution)/shard_map/ppermute | solution.py:353
  4.9 7.1 %collective-permute-start.1 = (bf16[16,2048]{1,0:T(8,128)(2,1)S(1)}, bf16[16,2048]{1,0:T(8,128)(2,1)S(1)}, u32[]{:S(2)}, u32[]{:S(2)}) collective-permute-start(bf16[16,2048]{1,0:T(8,128)(2,1)S(1)} %slice.9), channel_id=1, source_target_pairs={{1,2},{3,4},{5,6},{7,8},{9,10},{11,12},{13,14},{15,16},{17,18},{19... | collective-permute-start | bytes 196616 | tf_op jit(solution)/shard_map/ppermute | solution.py:354
  6.2 5.8 %collective-permute-start = (bf16[192,2048]{1,0:T(8,128)(2,1)}, bf16[192,2048]{1,0:T(8,128)(2,1)S(1)}, u32[]{:S(2)}, u32[]{:S(2)}) collective-permute-start(bf16[192,2048]{1,0:T(8,128)(2,1)} %own_ref.1), channel_id=1, source_target_pairs={{0,1},{1,0},{2,3},{3,2},{4,5},{5,4},{6,7},{7,6},{8,9},{9,8},{10,11... | collective-permute-start | bytes 2359304 | tf_op jit(solution)/shard_map/ppermute | solution.py:351
  8.3 0.7 %copy-start.1 = (f32[2048]{0:T(1024)S(1)}, f32[2048]{0:T(1024)}, u32[]{:S(2)}) copy-start(f32[2048]{0:T(1024)} %param.14) | copy-start | bytes 24580
  9.0 3.0 %copy-start.2 = (f32[2048]{0:T(1024)S(1)}, f32[2048]{0:T(1024)}, u32[]{:S(2)}) copy-start(f32[2048]{0:T(1024)} %param.14) | copy-start | bytes 24580
  9.0 3.0 %copy-start.3 = (bf16[4,1024]{1,0:T(4,128)(2,1)S(1)}, bf16[4,1024]{1,0:T(4,128)(2,1)}, u32[]{:S(2)}) copy-start(bf16[4,1024]{1,0:T(4,128)(2,1)} %taps_ref.2) | copy-start | bytes 24580
  12.0 18.0 %copy-start.4 = (bf16[4,1024]{1,0:T(4,128)(2,1)S(1)}, bf16[4,1024]{1,0:T(4,128)(2,1)}, u32[]{:S(2)}) copy-start(bf16[4,1024]{1,0:T(4,128)(2,1)} %taps_ref.3) | copy-start | bytes 24580
  17.9 1.2 %copy-start.6 = (bf16[400,2048]{1,0:T(8,128)(2,1)}, bf16[400,2048]{1,0:T(8,128)(2,1)S(1)}, u32[]{:S(2)}) copy-start(bf16[400,2048]{1,0:T(8,128)(2,1)S(1)} %get-tuple-element.43.rows_ref) | copy-start | bytes 4915204
  19.1 21.8 %all-to-all-start = ((bf16[64,8,384]{2,1,0:T(8,128)(2,1)}), bf16[64,8,384]{2,1,0:T(8,128)(2,1)S(1)}, u32[]{:S(2)}, u32[]{:S(2)}) async-start(bf16[64,8,384]{2,1,0:T(8,128)(2,1)} %bitcast.1), calls=%async_computation | async-start | bytes 786432 | tf_op jit(solution)/shard_map/all_to_all | solution.py:388
  30.0 1.4 %copy-start.7 = (bf16[400,2048]{1,0:T(8,128)(2,1)S(1)}, bf16[400,2048]{1,0:T(8,128)(2,1)}, u32[]{:S(2)}) copy-start(bf16[400,2048]{1,0:T(8,128)(2,1)} %copy-done.6) | copy-start | bytes 4915204
  31.4 17.4 %copy-start.5 = (f32[2048]{0:T(1024)S(1)}, f32[2048]{0:T(1024)}, u32[]{:S(2)}) copy-start(f32[2048]{0:T(1024)} %param.24) | copy-start | bytes 24580
  42.9 16.2 %all-to-all-start.1 = ((bf16[64,8,384]{2,1,0:T(8,128)(2,1)}), bf16[64,8,384]{2,1,0:T(8,128)(2,1)S(1)}, u32[]{:S(2)}, u32[]{:S(2)}) async-start(bf16[64,8,384]{2,1,0:T(8,128)(2,1)} %bitcast.4), calls=%async_computation.1 | async-start | bytes 786432 | tf_op jit(solution)/shard_map/all_to_all | solution.py:401
  48.8 1.4 %copy-start.8 = (bf16[400,2048]{1,0:T(8,128)(2,1)S(1)}, bf16[400,2048]{1,0:T(8,128)(2,1)}, u32[]{:S(2)}) copy-start(bf16[400,2048]{1,0:T(8,128)(2,1)} %copy-done.6) | copy-start | bytes 4915204
  63.0 4.6 %collective-permute-start.3 = (bf16[192,2048]{1,0:T(8,128)(2,1)S(1)}, bf16[192,2048]{1,0:T(8,128)(2,1)S(1)}, u32[]{:S(2)}, u32[]{:S(2)}) collective-permute-start(bf16[192,2048]{1,0:T(8,128)(2,1)S(1)} %get-tuple-element.48), channel_id=1, source_target_pairs={{0,1},{1,0},{2,3},{3,2},{4,5},{5,4},{6,7},{7,6},{8,9},{9,8},{10,11... | collective-permute-start | bytes 2359304 | tf_op jit(solution)/shard_map/ppermute | solution.py:414
